TPU v7x, 512 devices: a 4x2x32 block of a 4x8x32 slice. The times are simulated.
512 devices in a mesh: grp: 2 (over y), kv: 64 (over z, core), tp: 4 (over x).
Axes of the slice: x: 4, y: 2, z: 32, core: 2. Of those that a mesh axis runs over, the one named last changes fastest.
The devices are a block of a 4x8x32 slice.
Arguments:
- tokens: bfloat16 [65536, 2048], P(('grp', 'kv'), 'tp'), parts along dimension 0, may hold values from -5400 to 5400, as said below
- gain: bfloat16 [2048], replicated, may hold values from 0.099609375 to 1.8984375
- w_query: bfloat16 [2048, 1024], P(None, 'tp'), may hold values from -1 to 1
- w_key: bfloat16 [2048, 512], P(None, 'tp'), may hold values from -3 to 3
- w_value: bfloat16 [2048, 512], P(None, 'tp'), may hold values from -0.125 to 0.125
- w_out: bfloat16 [1024, 2048], P(None, 'tp'), may hold values from -2 to 2
- select: int32 [512, 32], P(('grp', 'kv')), parts along dimension 0, may hold values from -1 to 1023, as said below
Outputs:
- mixed: bfloat16 [65536, 2048], P(('grp', 'kv'), 'tp'), parts along dimension 0
There are 2 independent parts, one for each index of `grp`. A program takes and returns all parts, laid end to end along the dimension named above; an argument that names none is the same for every part. Nothing has to cross between parts.
Inputs may be any that keep to these rules, and one draw needn't show every extreme that they name: Entries of tokens are finite with scales that vary by row and by column. `select`: row b lists distinct key blocks that start no later than query block b ends, or -1 for an empty slot. Every query block lists each key block of its own index of kv up to its own last position. Apart from its own index, the query blocks of one index of kv together list at most 2 distinct key blocks held by any other index; every index but the first lists exactly 2 blocks of the index before it.
All inputs are finite; a program needn't handle non-finite values.
Results may differ from a plain program's by a relative error of at most 0.012.
Values may be sent and summed in bfloat16 or wider, within the bound.
A program may use at most 128 MiB of HBM per device.

v0:
```python
import jax
import jax.numpy as jnp
from jax import lax
from jax.sharding import PartitionSpec as P

HD = 128
QB = 128
KB = 32


epsilon = 1e-06
theta = 10000.0


def laid_out(blocks, dim):
    shape = list(blocks.shape[1:])
    shape[dim] *= blocks.shape[0]
    return jnp.moveaxis(blocks, 0, dim).reshape(shape)


def sent_to_all(array, axis):
    copies = jnp.broadcast_to(array, (lax.axis_size(axis), *array.shape))
    return lax.all_to_all(copies, axis, split_axis=0, concat_axis=0, tiled=True)


def gathered_copies(array, axis, dim):
    return laid_out(sent_to_all(array, axis), dim)


def side_by_side(arrays, axis, dim, along):
    ends, at = ([], 0)
    for a in arrays[:-1]:
        at += a.shape[along]
        ends.append(at)
    both = jnp.concatenate(arrays, axis=along)
    return tuple(jnp.split(lax.all_gather(both, axis, axis=dim, tiled=True), ends, axis=along))


def rotary(values, positions):
    head_width = values.shape[-1]
    frequency = theta ** (-jnp.arange(0, head_width, 2, dtype=jnp.float32) / head_width)
    angles = positions.astype(jnp.float32)[:, None] * frequency[None, :]
    cosine = jnp.cos(angles)[:, None, :]
    sine_table = jnp.sin(angles)[:, None, :]
    front_half = values[..., : head_width // 2]
    second = values[..., head_width // 2 :]
    return jnp.concatenate(
        [front_half * cosine - second * sine_table, second * cosine + front_half * sine_table],
        axis=-1,
    )


def per_device(tokens, gain, w_query, w_key, w_value, w_out, select):
    tok_rows = tokens.shape[0]
    model_width = gain.shape[0]
    my_index = lax.axis_index("kv")
    kv_local = w_key.shape[1] // HD
    group_size = w_query.shape[1] // w_key.shape[1]
    gain_f32 = gain.astype(jnp.float32)
    piece_f32 = gathered_copies(tokens, "tp", 1).astype(jnp.float32)
    scaled = (piece_f32 * gain_f32[None, :]).astype(jnp.bfloat16)
    acc_q = jnp.dot(scaled, w_query, preferred_element_type=jnp.float32)
    acc_k = jnp.dot(scaled, w_key, preferred_element_type=jnp.float32)
    acc_v = jnp.dot(scaled, w_value, preferred_element_type=jnp.float32)
    squares = jnp.sum(piece_f32 * piece_f32, axis=1)
    inverse = lax.rsqrt(squares / model_width + epsilon)[:, None]
    positions = my_index * tok_rows + jnp.arange(tok_rows, dtype=jnp.int32)
    queries = rotary((acc_q * inverse).reshape(tok_rows, -1, HD), positions).astype(jnp.bfloat16)
    keys_here = rotary((acc_k * inverse).reshape(tok_rows, kv_local, HD), positions).astype(
        jnp.bfloat16
    )
    values_here = (acc_v * inverse).astype(jnp.bfloat16).reshape(tok_rows, kv_local, HD)
    safe_ids = jnp.maximum(select, 0)
    keys_every, values_every = side_by_side((keys_here, values_here), "kv", 0, 1)
    table_k = keys_every.reshape(-1, KB, kv_local, HD)
    table_v = values_every.reshape(-1, KB, kv_local, HD)
    query_blocks = select.shape[0]
    chosen_count = select.shape[1]
    keys_sel = jnp.take(table_k, safe_ids, axis=0).reshape(
        query_blocks, chosen_count * KB, kv_local, HD
    )
    values_sel = jnp.take(table_v, safe_ids, axis=0).reshape(
        query_blocks, chosen_count * KB, kv_local, HD
    )
    query_rows = queries.reshape(query_blocks, QB, kv_local, group_size, HD)
    scores = jnp.einsum(
        "bqgrd,bkgd->bgrqk", query_rows, keys_sel, preferred_element_type=jnp.float32
    ) * HD ** (-0.5)
    key_pos = (safe_ids[:, :, None] * KB + jnp.arange(KB, dtype=jnp.int32)[None, None, :]).reshape(
        query_blocks, -1
    )
    live_keys = jnp.repeat(select >= 0, KB, axis=1)
    q_pos = positions.reshape(query_blocks, QB)
    allowed = live_keys[:, None, :] & (key_pos[:, None, :] <= q_pos[:, :, None])
    scores = jnp.where(allowed[:, None, None], scores, -jnp.inf)
    row_max = jnp.max(scores, axis=-1, keepdims=True)
    raised = jnp.exp(scores - row_max)
    weights = (raised / jnp.sum(raised, axis=-1, keepdims=True)).astype(jnp.bfloat16)
    attended = jnp.einsum(
        "bgrqk,bkgd->bqgrd", weights, values_sel, preferred_element_type=jnp.float32
    )
    attended = attended.astype(jnp.bfloat16).reshape(tok_rows, -1)
    mixed = jnp.dot(gathered_copies(attended, "tp", 1), w_out, preferred_element_type=jnp.float32)
    return mixed.astype(jnp.bfloat16)


def solution(mesh):
    placed = (
        P(("grp", "kv"), "tp"),
        P(),
        P(None, "tp"),
        P(None, "tp"),
        P(None, "tp"),
        P(None, "tp"),
        P(("grp", "kv"), None),
    )
    return jax.shard_map(
        per_device, mesh=mesh, in_specs=placed, out_specs=P(("grp", "kv"), "tp"), check_vma=False
    )
```

profile of v0, /device:TPU:33, one launch (start us, length us, event | category | flops | bytes accessed | tf_op | source)
XLA Modules:
  0.0 294.2 jit_solution(1347710809671723820)
XLA Ops:
  6.5 0.0 copy-start
  6.6 0.0 copy-start.5
  6.6 1.4 copy.12
  7.9 1.5 broadcast_in_dim.23
  9.4 5.1 %all-to-all-start = ((bf16[4,512,512]{1,2,0:T(8,128)(2,1)}), bf16[4,512,512]{1,2,0:T(8,128)(2,1)S(1)}, u32[]{:S(2)}, u32[]{:S(2)}) async-start(bf16[4,512,512]{1,2,0:T(8,128)(2,1)} %broadcast_in_dim.23), calls=%async_computation | async-start | bytes 4194304 | tf_op jit(solution)/shard_map/all_to_all | solution.py:23
  14.5 0.0 all-gather.2.cloned.1.call-start
  14.5 0.0 copy-done.5
  14.6 15.3 %all-to-all-done = bf16[4,512,512]{1,2,0:T(8,128)(2,1)S(1)} async-done(((bf16[4,512,512]{1,2,0:T(8,128)(2,1)}), bf16[4,512,512]{1,2,0:T(8,128)(2,1)S(1)}, u32[]{:S(2)}, u32[]{:S(2)}) %all-to-all-start) | async-done | bytes 2097184 | tf_op jit(solution)/shard_map/all_to_all | solution.py:23
  29.9 0.0 copy-start.7
  29.9 0.0 copy-start.8
  29.9 0.5 multiply_reduce_fusion
  30.4 0.5 fusion
  30.9 0.1 copy-done.7
  30.9 0.0 copy-start.2
  30.9 0.0 copy-start.4
  30.9 0.0 copy-start.6
  30.9 0.5 fusion.14
  31.4 0.8 copy-done.2
  32.2 0.0 copy-done.8
  32.2 0.5 fusion.9
  32.7 0.6 fusion.24
  33.3 0.7 pad_maximum_fusion
  34.0 0.1 all-gather.2.cloned.1.call-update
  34.1 0.0 copy-done.4
  34.1 0.1 reshape.281
  34.2 0.1 broadcast_in_dim.24
  34.3 0.1 and.19
  34.4 0.1 add.75
  34.5 0.1 add.72
  34.6 0.1 add.73
  34.7 0.5 multiply_cosine_fusion
  35.2 2.4 compare_and_fusion
  37.6 0.0 copy-done.6
  37.6 2.4 convolution_multiply_fusion
  40.0 0.1 subtract_convert_fusion
  40.1 0.2 copy.16
  40.4 0.9 copy.17
  41.2 178.9 %all-gather.2.cloned.1.call-done = bf16[32768,2,128]{0,2,1:T(8,128)(2,1)} async-done(((bf16[512,2,128]{0,2,1:T(8,128)(2,1)}), bf16[32768,2,128]{0,2,1:T(8,128)(2,1)}) %all-gather.2.cloned.1.call-update) | async-done | bytes 16777232 | tf_op jit(solution)/shard_map/all_gather | solution.py:36
  220.1 11.3 %fusion.30 = (bf16[32768,1,128]{0,2,1:T(8,128)(2,1)}, bf16[32768,1,128]{0,2,1:T(8,128)(2,1)}) fusion(bf16[32768,2,128]{0,2,1:T(8,128)(2,1)} %all-gather.2.cloned.1.call-done), kind=kLoop, calls=%fused_computation.58 | loop fusion | bytes 33554432 | tf_op jit(solution)/shard_map/split | solution.py:36
  231.4 11.9 %copy.15 = bf16[32768,1,128]{2,0,1:T(8,128)(2,1)} copy(bf16[32768,1,128]{0,2,1:T(8,128)(2,1)} %get-tuple-element.6) | data formatting | bytes 16777216 | tf_op jit(solution)/shard_map/split | solution.py:36
  243.3 11.4 %copy.14 = bf16[32768,1,128]{2,0,1:T(8,128)(2,1)} copy(bf16[32768,1,128]{0,2,1:T(8,128)(2,1)} %get-tuple-element.7) | data formatting | bytes 16777216 | tf_op jit(solution)/shard_map/split | solution.py:36
  254.7 4.1 %gather_fusion.1 = bf16[128,32,128]{2,1,0:T(8,128)(2,1)S(1)} fusion(bf16[1024,32,128]{2,1,0:T(8,128)(2,1)} %bitcast.81, s32[1024]{0:T(1024)S(1)} %pad_clamp_fusion), kind=kCustom, calls=%fused_computation.1.clone | custom fusion | bytes 2097664 | tf_op jit(solution)/shard_map/jit(_take)/gather | solution.py:79
  258.9 4.1 %gather_fusion = bf16[128,32,128]{2,1,0:T(8,128)(2,1)S(1)} fusion(bf16[1024,32,128]{2,1,0:T(8,128)(2,1)} %bitcast.82, s32[1024]{0:T(1024)S(1)} %pad_clamp_fusion), kind=kCustom, calls=%fused_computation.clone | custom fusion | bytes 2097664 | tf_op jit(solution)/shard_map/jit(_take)/gather | solution.py:82
  263.0 0.0 copy-start.1
  263.0 0.0 copy-start.3
  263.0 0.3 broadcast_select_fusion
  263.3 0.8 copy-done.1
  264.0 0.1 copy-done.3
  264.1 0.8 fusion.2
  264.9 1.0 fusion.1
  265.9 1.3 fusion.10
  267.3 0.2 copy.28
  267.5 0.1 broadcast_in_dim.31
  267.6 18.2 %all_to_all.10 = bf16[4,512,256]{1,2,0:T(8,128)(2,1)S(1)} all-to-all(bf16[4,512,256]{1,2,0:T(8,128)(2,1)S(1)} %broadcast_in_dim.31), channel_id=1, replica_groups=mesh['grp'=2,'kv'=64,'tp'=4] {'tp'}, dimensions={0} | all-to-all | bytes 2097152 | tf_op jit(solution)/shard_map/all_to_all | solution.py:23
  285.8 0.0 copy-done
  285.8 1.5 convolution_convert_fusion
  (13 shorter events, 0.2 us)
Async XLA Ops:
  6.5 279.3 %copy-start = (bf16[1024,512]{1,0:T(8,128)(2,1)S(1)}, bf16[1024,512]{1,0:T(8,128)(2,1)}, u32[]{:S(2)}) copy-start(bf16[1024,512]{1,0:T(8,128)(2,1)} %param.14) | copy-start | bytes 3145732
  6.6 8.0 %copy-start.5 = (bf16[2048]{0:T(1024)(128)(2,1)S(1)}, bf16[2048]{0:T(1024)(128)(2,1)}, u32[]{:S(2)}) copy-start(bf16[2048]{0:T(1024)(128)(2,1)} %param.10) | copy-start | bytes 12292
  9.4 20.5 %all-to-all-start = ((bf16[4,512,512]{1,2,0:T(8,128)(2,1)}), bf16[4,512,512]{1,2,0:T(8,128)(2,1)S(1)}, u32[]{:S(2)}, u32[]{:S(2)}) async-start(bf16[4,512,512]{1,2,0:T(8,128)(2,1)} %broadcast_in_dim.23), calls=%async_computation | async-start | bytes 4194304 | tf_op jit(solution)/shard_map/all_to_all | solution.py:23
  14.5 205.6 %all-gather.2.cloned.1.call-start = ((), (), s32[]{:S(2)}) async-start(), calls=%async_computation.2 | async-start | bytes 17039360 | tf_op jit(solution)/shard_map/all_gather | solution.py:36
  29.9 1.0 copy-start.7
  29.9 2.4 copy-start.8
  30.9 1.3 copy-start.2
  30.9 3.2 %copy-start.4 = (s32[4,32]{1,0:T(4,128)S(1)}, s32[4,32]{1,0:T(4,128)}, u32[]{:S(2)}) copy-start(s32[4,32]{1,0:T(4,128)} %param.15) | copy-start | bytes 1540
  30.9 6.7 %copy-start.6 = (bf16[2048,256]{1,0:T(8,128)(2,1)S(1)}, bf16[2048,256]{1,0:T(8,128)(2,1)}, u32[]{:S(2)}) copy-start(bf16[2048,256]{1,0:T(8,128)(2,1)} %param.11) | copy-start | bytes 3145732
  263.0 1.0 copy-start.1
  263.0 1.1 copy-start.3
Sparse Core Ops, SparseCore 0:
  34.2 185.8 all-gather.1
where the time goes:
time: 295 us; the launch traced here: 294 us
  waiting for transfers between devices  194 us (66%)
  local copies, waits for them, and re-layouts  49.4 us (17%)
  blocking collectives  18.2 us (6%)
  between operations  13.6 us (5%)
  matrix products  7.03 us (2%)
  other arithmetic  6.52 us (2%)
  starting transfers between devices  5.12 us (2%)
    all_gather x1, waiting for transfers between devices, side_by_side(): lax.all_gather(both, axis, axis=dim, tiled=True)  179 us
    split x3, local copies, waits for them, and re-layouts, side_by_side(): jnp.split(lax.all_gather(both, axis, axis=dim, tiled=True), ends, axis=al...  34.6 us
    all_to_all x1, blocking collectives, sent_to_all(): return lax.all_to_all(copies, axis, split_axis=0, concat_axis=0, tiled=True)  18.2 us
    all_to_all x1, waiting for transfers between devices, sent_to_all(): return lax.all_to_all(copies, axis, split_axis=0, concat_axis=0, tiled=True)  15.3 us
  transfers between devices with their start and end apart: 2, of which 2 were waited for; matrix products, arithmetic and copies ran while one was open for 2% of the time, Pallas kernels for 0%

commit v1 on v0

v1 whole, which is shorter than its diff:
```python
import functools

import jax
import jax.numpy as jnp
from jax import lax
from jax.experimental import pallas as pl
from jax.experimental.pallas import tpu as pltpu
from jax.sharding import PartitionSpec as P

HD = 128
QB = 128
KB = 32
PIECES = 4

epsilon = 1e-06
theta = 10000.0
MESH = pl.DeviceIdType.MESH


def rotary_tables(positions):
    frequency = theta ** (-jnp.arange(0, HD, 2, dtype=jnp.float32) / HD)
    angles = positions.astype(jnp.float32)[:, None] * frequency[None, :]
    cosine, sine = jnp.cos(angles), jnp.sin(angles)
    return jnp.concatenate([cosine, cosine], 1), jnp.concatenate([-sine, sine], 1)


def remote(src, dst, send, recv, **where):
    return pltpu.make_async_remote_copy(
        src_ref=src, dst_ref=dst, send_sem=send, recv_sem=recv, device_id=where, device_id_type=MESH
    )


class TpRing:
    def __init__(self, own, slots, send, recv, rows):
        self.n = lax.axis_size("tp")
        self.me = lax.axis_index("tp")
        self.right = lax.rem(self.me + 1, self.n)
        self.left = lax.rem(self.me + self.n - 1, self.n)
        self.far = lax.rem(self.me + 2, self.n)
        self.own, self.slots, self.send, self.recv, self.rows = own, slots, send, recv, rows

    def copy(self, chunk, kind):
        half = self.rows // 2
        start, size, source, to = {
            0: (0, self.rows, None, self.right),
            1: (0, self.rows, None, self.left),
            2: (0, half, self.left, self.right),
            3: (half, half, self.right, self.left),
        }[kind]
        at = pl.ds(chunk * self.rows + start, size)
        src = self.own.at[at] if source is None else self.slots.at[source, at]
        dst = self.slots.at[self.me if source is None else source, at]
        return remote(src, dst, self.send.at[chunk, kind], self.recv.at[chunk, kind], tp=to)

    def begin(self, chunk):
        self.copy(chunk, 0).start()
        self.copy(chunk, 1).start()

    def hand_on(self, chunk):
        self.copy(chunk, 0).wait_recv()
        self.copy(chunk, 2).start()
        self.copy(chunk, 1).wait_recv()
        self.copy(chunk, 3).start()

    def arrived(self, chunk):
        self.copy(chunk, 2).wait_recv()
        self.copy(chunk, 3).wait_recv()

    def sent(self, chunk):
        for kind in range(4):
            self.copy(chunk, kind).wait_send()


def greet(others):
    barrier = pltpu.get_barrier_semaphore()
    for where in others:
        pl.semaphore_signal(barrier, inc=1, device_id=where, device_id_type=MESH)
    pl.semaphore_wait(barrier, len(others))


def project_kernel(
    tok, gain, wq, wk, wv, cos, sin, q_out, every,
    slots, weights, kv, send_t, recv_t, send_z, recv_z, send_c, recv_c, local,
):
    rows, width = tok.shape
    tp = lax.axis_size("tp")
    chunk_rows = rows // PIECES
    ring = TpRing(tok, slots, send_t, recv_t, chunk_rows)
    devices = lax.axis_size("kv")
    chips = devices // 2
    mine = lax.axis_index("kv")
    z, core = mine // 2, lax.rem(mine, 2)
    partner = mine + 1 - 2 * core
    up = lax.rem(mine + 2, devices)
    down = lax.rem(mine + devices - 2, devices)
    q_cols, k_cols = wq.shape[1], wk.shape[1]
    loads = [
        pltpu.make_async_copy(wq, weights.at[:, pl.ds(0, q_cols)], local.at[0]),
        pltpu.make_async_copy(wk, weights.at[:, pl.ds(q_cols, k_cols)], local.at[1]),
        pltpu.make_async_copy(wv, weights.at[:, pl.ds(q_cols + k_cols, k_cols)], local.at[2]),
        pltpu.make_async_copy(tok, slots.at[ring.me], local.at[3]),
    ]
    for load in loads:
        load.start()
    greet(
        [{"tp": ring.right}, {"tp": ring.left}, {"kv": partner}, {"kv": up}, {"kv": down}]
    )
    for chunk in range(PIECES):
        ring.begin(chunk)
    for load in loads:
        load.wait()

    def piece_of(owner, piece):
        return every.at[owner, pl.ds(piece * chunk_rows, chunk_rows)]

    def owner_at(direction, step):
        if direction == 0:
            return lax.rem(z - step + chips, chips) * 2 + core
        return lax.rem(z + step, chips) * 2 + core

    def hop(direction, step, piece):
        to = up if direction == 0 else down
        owner = owner_at(direction, step - 1)
        return remote(
            piece_of(owner, piece), piece_of(owner, piece),
            send_z.at[direction, step, piece], recv_z.at[direction, step, piece], kv=to,
        )

    def first_hop(direction, piece):
        to = up if direction == 0 else down
        return remote(
            kv.at[pl.ds(piece * chunk_rows, chunk_rows)], piece_of(mine, piece),
            send_z.at[direction, 1, piece], recv_z.at[direction, 1, piece], kv=to,
        )

    def across(direction, step, piece):
        owner = owner_at(direction, step)
        return remote(
            piece_of(owner, piece), piece_of(owner, piece),
            send_c.at[direction, step], recv_c.at[direction, step], kv=partner,
        )

    def across_whole(direction, step):
        owner = owner_at(direction, step)
        return remote(
            every.at[owner], every.at[owner],
            send_c.at[direction, step], recv_c.at[direction, step], kv=partner,
        )

    for chunk in range(PIECES):
        ring.hand_on(chunk)
        ring.arrived(chunk)
        at = pl.ds(chunk * chunk_rows, chunk_rows)
        total = jnp.zeros((chunk_rows, weights.shape[1]), jnp.float32)
        squares = jnp.zeros((chunk_rows, 1), jnp.float32)
        for t in range(tp):
            block = slots[t, at, :].astype(jnp.float32)
            squares += jnp.sum(block * block, axis=1, keepdims=True)
            scaled = (block * gain[:, t * width:(t + 1) * width].astype(jnp.float32)).astype(jnp.bfloat16)
            total += jnp.dot(
                scaled, weights[t * width:(t + 1) * width, :], preferred_element_type=jnp.float32
            )
        inverse = lax.rsqrt(squares / (tp * width) + epsilon)
        total *= inverse
        cosine, sine = cos[at, :], sin[at, :]
        heads = []
        for h in range((q_cols + k_cols) // HD):
            head = total[:, h * HD:(h + 1) * HD]
            heads.append((head * cosine + pltpu.roll(head, HD // 2, 1) * sine).astype(jnp.bfloat16))
        for h in range(q_cols // HD):
            q_out[at, h * HD:(h + 1) * HD] = heads[h]
        kv[at, 0:k_cols] = heads[-1]
        kv[at, k_cols:2 * k_cols] = total[:, q_cols + k_cols:].astype(jnp.bfloat16)
        first_hop(0, chunk).start()
        first_hop(1, chunk).start()

    keep = pltpu.make_async_copy(kv, every.at[mine], local.at[4])
    keep.start()
    give = remote(kv, every.at[mine], send_c.at[0, 0], recv_c.at[0, 0], kv=partner)
    give.start()

    last = chips // 2
    half = PIECES // 2

    @pl.loop(1, last - 1)
    def _(step):
        for piece in range(PIECES):
            for direction in range(2):
                hop(direction, step, piece).wait_recv()
                hop(direction, step + 1, piece).start()
                across(direction, step, piece).start()

    for piece in range(PIECES):
        for direction in range(2):
            hop(direction, last - 1, piece).wait_recv()
            if (piece < half) == (direction == 0):
                hop(direction, last, piece).start()
            across(direction, last - 1, piece).start()
    for piece in range(half):
        for direction in range(2):
            which = piece + direction * half
            hop(direction, last, which).wait_recv()
            across(0, last, which).start()

    keep.wait()
    give.wait()
    for chunk in range(PIECES):
        ring.sent(chunk)
        for direction in range(2):
            first_hop(direction, chunk).wait_send()

    @pl.loop(1, last)
    def _(step):
        for direction in range(2):
            across_whole(direction, step).wait()

    @pl.loop(2, last)
    def _(step):
        for direction in range(2):
            for piece in range(PIECES):
                hop(direction, step, piece).wait_send()

    across_whole(0, last).wait()
    for piece in range(half):
        for direction in range(2):
            hop(direction, last, piece + direction * half).wait_send()


def project(tokens, gain, w_query, w_key, w_value, cosine, sine):
    rows, width = tokens.shape
    devices = lax.axis_size("kv")
    tp = lax.axis_size("tp")
    q_cols, k_cols = w_query.shape[1], w_key.shape[1]
    steps = devices // 4 + 1
    dma = pltpu.SemaphoreType.DMA
    vmem = pl.BlockSpec(memory_space=pltpu.VMEM)
    hbm = pl.BlockSpec(memory_space=pl.ANY)
    return pl.pallas_call(
        project_kernel,
        out_shape=(
            jax.ShapeDtypeStruct((rows, q_cols), jnp.bfloat16),
            jax.ShapeDtypeStruct((devices, rows, 2 * k_cols), jnp.bfloat16),
        ),
        in_specs=[vmem, vmem, hbm, hbm, hbm, vmem, vmem],
        out_specs=(vmem, hbm),
        scratch_shapes=[
            pltpu.VMEM((tp, rows, width), jnp.bfloat16),
            pltpu.VMEM((tp * width, q_cols + 2 * k_cols), jnp.bfloat16),
            pltpu.VMEM((rows, 2 * k_cols), jnp.bfloat16),
            dma((PIECES, 4)),
            dma((PIECES, 4)),
            dma((2, steps, PIECES)),
            dma((2, steps, PIECES)),
            dma((2, steps)),
            dma((2, steps)),
            dma((5,)),
        ],
        compiler_params=pltpu.CompilerParams(collective_id=0, has_side_effects=True),
        name="project",
    )(tokens, gain, w_query, w_key, w_value, cosine, sine)


def attend_kernel(listed, q, sel, every, out, keys, sems):
    blocks, slots = sel.shape
    heads = q.shape[1] // HD
    start_at = lax.axis_index("kv") * q.shape[0]

    def fetch(b, s, index):
        return pltpu.make_async_copy(
            every.at[pl.ds(pl.multiple_of(index * KB, KB), KB)],
            keys.at[b, pl.ds(pl.multiple_of(s * KB, KB), KB)],
            sems.at[b],
        )

    for b in range(blocks):
        @pl.loop(0, slots)
        def _(s, b=b):
            fetch(b, s, jnp.maximum(listed[b, s], 0)).start()

    width = slots * KB
    spread = (
        lax.broadcasted_iota(jnp.int32, (slots, width), 1) // KB
        == lax.broadcasted_iota(jnp.int32, (slots, width), 0)
    ).astype(jnp.float32)
    ids = sel[...]
    safe = jnp.where(ids < 0, 1 << 20, ids)
    high = (safe // 64).astype(jnp.float32)
    low = lax.rem(safe, 64).astype(jnp.float32)
    wide = jnp.dot(high, spread, preferred_element_type=jnp.float32) * 64.0 + jnp.dot(
        low, spread, preferred_element_type=jnp.float32
    )
    key_pos = wide.astype(jnp.int32) * KB + lax.rem(
        lax.broadcasted_iota(jnp.int32, (blocks, width), 1), KB
    )
    for b in range(blocks):
        pltpu.make_async_copy(every.at[pl.ds(0, width)], keys.at[b], sems.at[b]).wait()
        q_pos = start_at + b * QB + lax.broadcasted_iota(jnp.int32, (QB, width), 0)
        allowed = jnp.broadcast_to(key_pos[b:b + 1, :], (QB, width)) <= q_pos
        for h in range(heads):
            score = lax.dot_general(
                q[b * QB:(b + 1) * QB, h * HD:(h + 1) * HD], keys[b, :, 0:HD],
                (((1,), (1,)), ((), ())), preferred_element_type=jnp.float32,
            ) * HD ** (-0.5)
            score = jnp.where(allowed, score, -jnp.inf)
            raised = jnp.exp(score - jnp.max(score, axis=1, keepdims=True))
            weights = (raised / jnp.sum(raised, axis=1, keepdims=True)).astype(jnp.bfloat16)
            out[b * QB:(b + 1) * QB, h * HD:(h + 1) * HD] = jnp.dot(
                weights, keys[b, :, HD:2 * HD], preferred_element_type=jnp.float32
            ).astype(jnp.bfloat16)


def attend(select, queries, every):
    blocks, slots = select.shape
    rows, cols = queries.shape
    vmem = pl.BlockSpec(memory_space=pltpu.VMEM)
    return pl.pallas_call(
        attend_kernel,
        out_shape=jax.ShapeDtypeStruct((rows, cols), jnp.bfloat16),
        in_specs=[
            pl.BlockSpec(memory_space=pltpu.SMEM), vmem, vmem, pl.BlockSpec(memory_space=pl.ANY)
        ],
        out_specs=vmem,
        scratch_shapes=[
            pltpu.VMEM((blocks, slots * KB, 2 * HD), jnp.bfloat16),
            pltpu.SemaphoreType.DMA((blocks,)),
        ],
        name="attend",
    )(select, queries, select, every)


def mix_kernel(mine, w_out, out, slots, send_t, recv_t, local):
    rows, width = mine.shape
    chunk_rows = rows // PIECES
    ring = TpRing(mine, slots, send_t, recv_t, chunk_rows)
    keep = pltpu.make_async_copy(mine, slots.at[ring.me], local)
    keep.start()
    greet([{"tp": ring.right}, {"tp": ring.left}])
    for chunk in range(PIECES):
        ring.begin(chunk)
    keep.wait()
    for chunk in range(PIECES):
        ring.hand_on(chunk)
        ring.arrived(chunk)
        at = pl.ds(chunk * chunk_rows, chunk_rows)
        total = jnp.zeros((chunk_rows, out.shape[1]), jnp.float32)
        for t in range(lax.axis_size("tp")):
            total += jnp.dot(
                slots[t, at, :], w_out[t * width:(t + 1) * width, :],
                preferred_element_type=jnp.float32,
            )
        out[at, :] = total.astype(jnp.bfloat16)
    for chunk in range(PIECES):
        ring.sent(chunk)


def mix(attended, w_out):
    rows, width = attended.shape
    tp = lax.axis_size("tp")
    dma = pltpu.SemaphoreType.DMA
    vmem = pl.BlockSpec(memory_space=pltpu.VMEM)
    return pl.pallas_call(
        mix_kernel,
        out_shape=jax.ShapeDtypeStruct((rows, w_out.shape[1]), jnp.bfloat16),
        in_specs=[vmem, vmem],
        out_specs=vmem,
        scratch_shapes=[
            pltpu.VMEM((tp, rows, width), jnp.bfloat16),
            dma((PIECES, 4)),
            dma((PIECES, 4)),
            dma(()),
        ],
        compiler_params=pltpu.CompilerParams(collective_id=1, has_side_effects=True),
        name="mix",
    )(attended, w_out)


def per_device(tokens, gain, w_query, w_key, w_value, w_out, select):
    rows = tokens.shape[0]
    positions = lax.axis_index("kv") * rows + jnp.arange(rows, dtype=jnp.int32)
    cosine, sine = rotary_tables(positions)
    queries, every = project(
        tokens, gain.reshape(1, -1), w_query, w_key, w_value, cosine, sine
    )
    attended = attend(select, queries, every.reshape(-1, every.shape[2]))
    return mix(attended, w_out)


def solution(mesh):
    placed = (
        P(("grp", "kv"), "tp"),
        P(),
        P(None, "tp"),
        P(None, "tp"),
        P(None, "tp"),
        P(None, "tp"),
        P(("grp", "kv"), None),
    )
    return jax.shard_map(
        per_device, mesh=mesh, in_specs=placed, out_specs=P(("grp", "kv"), "tp"), check_vma=False
    )
```

time: 295 us -> 204 us (0.69)
  Pallas kernels: 0 us -> 196 us
  waiting for transfers between devices: 194 us -> 0 us
  local copies, waits for them, and re-layouts: 49.4 us -> 3.16 us
  blocking collectives: 18.2 us -> 0 us
  between operations: 13.6 us -> 0.04 us
  matrix products: 7.03 us -> 0 us
  starting transfers between devices: 5.12 us -> 0 us
  other arithmetic: 6.52 us -> 1.99 us
    pallas_call x0 -> x3, Pallas kernels: none -> 196 us  [the longest x1 167 us: project(): pl.pallas_call(project_kernel, out_shape=(jax.ShapeDtypeStruct((rows, q_c...]
    all_gather x1 -> x0, waiting for transfers between devices: 179 us -> none  [side_by_side(): lax.all_gather(both, axis, axis=dim, tiled=True)]
    split x3 -> x0, local copies, waits for them, and re-layouts: 34.6 us -> none  [side_by_side(): jnp.split(lax.all_gather(both, axis, axis=dim, tiled=True), ends, axis=al...]
    all_to_all x1 -> x0, blocking collectives: 18.2 us -> none  [sent_to_all(): return lax.all_to_all(copies, axis, split_axis=0, concat_axis=0, tiled=True)]
    all_to_all x1 -> x0, waiting for transfers between devices: 15.3 us -> none  [sent_to_all(): return lax.all_to_all(copies, axis, split_axis=0, concat_axis=0, tiled=True)]
    gather x2 -> x0, local copies, waits for them, and re-layouts: 8.27 us -> none  [the longest x1 4.14 us: per_device(): jnp.take(table_v, safe_ids, axis=0)]
    dot_general x6 -> x0, matrix products: 7.03 us -> none  [the longest x1 2.35 us: per_device(): acc_q = jnp.dot(scaled, w_query, preferred_element_type=jnp.float32)]
    all_to_all x1 -> x0, starting transfers between devices: 5.12 us -> none  [sent_to_all(): return lax.all_to_all(copies, axis, split_axis=0, concat_axis=0, tiled=True)]
  transfers between devices with their start and end apart: 2 -> 0, of which waited for: 2 -> 0; matrix products, arithmetic and copies ran while one was open for 2% -> 0% of each run, Pallas kernels for 0% -> 0%
where the time goes in v1:
time: 204 us; the launch traced here: 202 us
  Pallas kernels  196 us (96%)
  local copies, waits for them, and re-layouts  3.16 us (2%)
    pallas_call x1, Pallas kernels, project(): pl.pallas_call(project_kernel, out_shape=(jax.ShapeDtypeStruct((rows, q_c...  167 us
    pallas_call x1, Pallas kernels, mix(): pl.pallas_call(mix_kernel, out_shape=jax.ShapeDtypeStruct((rows, w_out.sh...  22.2 us
    pallas_call x1, Pallas kernels, attend(): pl.pallas_call(attend_kernel, out_shape=jax.ShapeDtypeStruct((rows, cols)...  7.75 us

profile of v1, /device:TPU:33, one launch (start us, length us, event | category | flops | bytes accessed | tf_op | source)
XLA Modules:
  0.0 201.7 jit_solution(11254317324819202590)
XLA Ops:
  0.0 1.3 reshape.18.gain
  1.3 1.0 fusion
  2.3 1.0 pad_maximum_fusion
  3.3 166.6 %project.1 = (bf16[512,256]{1,0:T(8,128)(2,1)}, bf16[64,512,256]{2,1,0:T(8,128)(2,1)}) custom-call(bf16[512,512]{1,0:T(8,128)(2,1)} %tok.1, bf16[1,2048]{1,0:T(2,128)(2,1)} %reshape.18.gain, bf16[2048,256]{1,0:T(8,128)(2,1)} %wq.1, bf16[2048,128]{1,0:T(8,128)(2,1)} %wk.1, bf16[2048,128]{1,0:T(8,128)(2,1)} %wv.1, f32[512,128]{1,0:T(8,128)} %get-tuple-element.12.cos, ...), custom_call_target="tpu_custom_call" | custom-call | tf_op jit(solution)/shard_map/project/pallas_call | solution.py:238
  169.9 7.7 %attend.1.mine = bf16[512,256]{1,0:T(8,128)(2,1)} custom-call(s32[4,32]{1,0:T(4,128)} %sel.1, bf16[512,256]{1,0:T(8,128)(2,1)} %get-tuple-element.7.q, s32[4,32]{1,0:T(4,128)} %sel.1, bf16[32768,256]{1,0:T(8,128)(2,1)} %bitcast.1), custom_call_target="tpu_custom_call" | custom-call | tf_op jit(solution)/shard_map/attend/pallas_call | solution.py:316
  177.6 22.2 %mix.1 = bf16[512,512]{1,0:T(8,128)(2,1)} custom-call(bf16[512,256]{1,0:T(8,128)(2,1)} %attend.1.mine, bf16[1024,512]{1,0:T(8,128)(2,1)} %w_out.1), custom_call_target="tpu_custom_call" | custom-call | tf_op jit(solution)/shard_map/mix/pallas_call | solution.py:361
  199.8 1.9 copy.9
  (2 shorter events, 0.0 us)

commit v2 on v0

v2 whole, which is shorter than its diff:
```python
import functools

import jax
import jax.numpy as jnp
from jax import lax
from jax.experimental import pallas as pl
from jax.experimental.pallas import tpu as pltpu
from jax.sharding import PartitionSpec as P

HD = 128
QB = 128
KB = 32
PIECES = 4

epsilon = 1e-06
theta = 10000.0
MESH = pl.DeviceIdType.MESH


def rotary_tables(positions):
    frequency = theta ** (-jnp.arange(0, HD, 2, dtype=jnp.float32) / HD)
    angles = positions.astype(jnp.float32)[:, None] * frequency[None, :]
    cosine, sine = jnp.cos(angles), jnp.sin(angles)
    return jnp.concatenate([cosine, cosine], 1), jnp.concatenate([-sine, sine], 1)


def remote(src, dst, send, recv, **where):
    return pltpu.make_async_remote_copy(
        src_ref=src, dst_ref=dst, send_sem=send, recv_sem=recv, device_id=where, device_id_type=MESH
    )


class TpRing:
    def __init__(self, own, slots, send, recv, rows):
        self.n = lax.axis_size("tp")
        self.me = lax.axis_index("tp")
        self.right = lax.rem(self.me + 1, self.n)
        self.left = lax.rem(self.me + self.n - 1, self.n)
        self.far = lax.rem(self.me + 2, self.n)
        self.own, self.slots, self.send, self.recv, self.rows = own, slots, send, recv, rows

    def copy(self, chunk, kind):
        half = self.rows // 2
        start, size, source, to = {
            0: (0, self.rows, None, self.right),
            1: (0, self.rows, None, self.left),
            2: (0, half, self.left, self.right),
            3: (half, half, self.right, self.left),
        }[kind]
        at = pl.ds(chunk * self.rows + start, size)
        src = self.own.at[at] if source is None else self.slots.at[source, at]
        dst = self.slots.at[self.me if source is None else source, at]
        return remote(src, dst, self.send.at[chunk, kind], self.recv.at[chunk, kind], tp=to)

    def begin(self, chunk):
        self.copy(chunk, 0).start()
        self.copy(chunk, 1).start()

    def hand_on(self, chunk):
        self.copy(chunk, 0).wait_recv()
        self.copy(chunk, 2).start()
        self.copy(chunk, 1).wait_recv()
        self.copy(chunk, 3).start()

    def arrived(self, chunk):
        self.copy(chunk, 2).wait_recv()
        self.copy(chunk, 3).wait_recv()

    def sent(self, chunk):
        for kind in range(4):
            self.copy(chunk, kind).wait_send()


def layer_kernel(
    tok, gain, wq, wk, wv, w_out, cos, sin, listed, sel, out,
    slots, weights, queries, need, transit, keys, attended, mixing,
    send_t, recv_t, send_z, recv_z, send_c, recv_c, send_m, recv_m, local, go,
):
    rows, width = tok.shape
    tp = lax.axis_size("tp")
    chunk_rows = rows // PIECES
    devices = lax.axis_size("kv")
    chips = devices // 2
    most_up, most_down = reach(chips)
    mine = lax.axis_index("kv")
    z, core = mine // 2, lax.rem(mine, 2)
    partner = mine + 1 - 2 * core
    up = lax.rem(mine + 2, devices)
    down = lax.rem(mine + devices - 2, devices)
    q_cols, k_cols = wq.shape[1], wk.shape[1]
    ring = TpRing(tok, slots, send_t, recv_t, chunk_rows)
    mix_ring = TpRing(attended, mixing, send_m, recv_m, chunk_rows)

    loads = [
        pltpu.make_async_copy(wq, weights.at[:, pl.ds(0, q_cols)], local.at[0]),
        pltpu.make_async_copy(wk, weights.at[:, pl.ds(q_cols, k_cols)], local.at[1]),
        pltpu.make_async_copy(wv, weights.at[:, pl.ds(q_cols + k_cols, k_cols)], local.at[2]),
        pltpu.make_async_copy(tok, slots.at[ring.me], local.at[3]),
    ]
    for load in loads:
        load.start()

    barrier = pltpu.get_barrier_semaphore()

    def hail(**where):
        pl.semaphore_signal(barrier, inc=1, device_id=where, device_id_type=MESH)

    hail(tp=ring.right)
    hail(tp=ring.left)
    hail(kv=partner)
    hail(kv=down)

    @pl.when(z < chips - 1)
    def _():
        hail(kv=up)

    @pl.when(z == 0)
    def _():
        pl.semaphore_wait(barrier, 4)

    @pl.when(z > 0)
    def _():
        pl.semaphore_wait(barrier, 5)

    @pl.when(z == chips - 1)
    def _():
        pl.semaphore_signal(go, inc=1, device_id={"kv": up}, device_id_type=MESH)

    own_blocks = rows // KB
    chunk_blocks = chunk_rows // KB

    def piece_rows(piece):
        return pl.ds(piece * chunk_rows, chunk_rows)

    def piece_blocks(holder, piece):
        return pl.ds(holder * own_blocks + piece * chunk_blocks, chunk_blocks)

    def goes_up(step):
        return (step <= most_up) & (z - step + 1 >= 0) & (z < chips - 1)

    def comes_up(step):
        return (step <= most_up) & (z - step >= 0)

    def goes_down(step):
        return (step <= most_down) & (lax.rem(z + step - 1, chips) < most_down)

    def comes_down(step):
        return (step <= most_down) & (lax.rem(z + step, chips) < most_down)

    def send_up(step, piece):
        block = need.at[piece_blocks(lax.rem(z - step + 1 + chips, chips) * 2 + core, piece)]
        return remote(block, block, send_z.at[0, step, piece], recv_z.at[0, step, piece], kv=up)

    def send_down(step, piece, from_transit, to_transit):
        chip = lax.rem(z + step - 1, chips)
        kept = need.at[piece_blocks(chip * 2 + core, piece)]
        passing = transit.at[piece_blocks(lax.rem(chip, most_down), piece)]
        return remote(
            passing if from_transit else kept, passing if to_transit else kept,
            send_z.at[1, step, piece], recv_z.at[1, step, piece], kv=down,
        )

    def across(direction, step, piece):
        chip = lax.rem(z - step + chips, chips) if direction == 0 else lax.rem(z + step, chips)
        block = need.at[piece_blocks(chip * 2 + core, piece)]
        return remote(
            block, block, send_c.at[direction, step], recv_c.at[direction, step], kv=partner
        )

    def across_whole(direction, step):
        block = need.at[pl.ds(mine * own_blocks, own_blocks)]
        return remote(
            block, block, send_c.at[direction, step], recv_c.at[direction, step], kv=partner
        )

    def project(chunk):
        at = piece_rows(chunk)
        total = jnp.zeros((chunk_rows, weights.shape[1]), jnp.float32)
        squares = jnp.zeros((chunk_rows, 1), jnp.float32)
        for t in range(tp):
            block = slots[t, at, :].astype(jnp.float32)
            squares += jnp.sum(block * block, axis=1, keepdims=True)
            scaled = (block * gain[:, t * width:(t + 1) * width].astype(jnp.float32)).astype(
                jnp.bfloat16
            )
            total += jnp.dot(
                scaled, weights[t * width:(t + 1) * width, :], preferred_element_type=jnp.float32
            )
        total *= lax.rsqrt(squares / (tp * width) + epsilon)
        cosine, sine = cos[at, :], sin[at, :]
        heads = []
        for h in range((q_cols + k_cols) // HD):
            head = total[:, h * HD:(h + 1) * HD]
            heads.append((head * cosine + pltpu.roll(head, HD // 2, 1) * sine).astype(jnp.bfloat16))
        for h in range(q_cols // HD):
            queries[at, h * HD:(h + 1) * HD] = heads[h]
        kept = piece_blocks(mine, chunk)
        values = total[:, q_cols + k_cols:].astype(jnp.bfloat16)
        need[kept, :, 0:k_cols] = heads[-1].reshape(chunk_blocks, KB, k_cols)
        need[kept, :, k_cols:2 * k_cols] = values.reshape(chunk_blocks, KB, k_cols)

        @pl.when(goes_up(1))
        def _():
            send_up(1, chunk).start()

        @pl.when(goes_down(1) & (z > 0))
        def _():
            send_down(1, chunk, False, True).start()

    ring.begin(0)
    ring.begin(1)
    for load in loads:
        load.wait()
    for chunk in range(PIECES):
        if chunk == 0:
            ring.hand_on(0)
            ring.begin(2)
            ring.hand_on(1)
            ring.begin(3)
        elif chunk + 1 < PIECES:
            ring.hand_on(chunk + 1)
        ring.arrived(chunk)
        project(chunk)
    give = across_whole(0, 0)
    give.start()

    blocks, listed_slots = sel.shape
    wide = listed_slots * KB
    heads_here = q_cols // HD

    def attend(b, key_pos):
        @pl.loop(0, listed_slots, unroll=4)
        def _(s):
            keys[pl.ds(pl.multiple_of(s * KB, KB), KB), :] = need[jnp.maximum(listed[b, s], 0)]

        q_pos = mine * rows + b * QB + lax.broadcasted_iota(jnp.int32, (QB, wide), 0)
        allowed = jnp.broadcast_to(key_pos[b:b + 1, :], (QB, wide)) <= q_pos
        for h in range(heads_here):
            score = lax.dot_general(
                queries[b * QB:(b + 1) * QB, h * HD:(h + 1) * HD], keys[:, 0:HD],
                (((1,), (1,)), ((), ())), preferred_element_type=jnp.float32,
            ) * HD ** (-0.5)
            score = jnp.where(allowed, score, -jnp.inf)
            raised = jnp.exp(score - jnp.max(score, axis=1, keepdims=True))
            parts = (raised / jnp.sum(raised, axis=1, keepdims=True)).astype(jnp.bfloat16)
            attended[b * QB:(b + 1) * QB, h * HD:(h + 1) * HD] = jnp.dot(
                parts, keys[:, HD:2 * HD], preferred_element_type=jnp.float32
            ).astype(jnp.bfloat16)
        mixing[mix_ring.me, b * QB:(b + 1) * QB, :] = attended[b * QB:(b + 1) * QB, :]

    def mix(chunk):
        at = piece_rows(chunk)
        total = jnp.zeros((chunk_rows, out.shape[1]), jnp.float32)
        for t in range(tp):
            total += jnp.dot(
                mixing[t, at, :], w_out[t * q_cols:(t + 1) * q_cols, :],
                preferred_element_type=jnp.float32,
            )
        out[at, :] = total.astype(jnp.bfloat16)

    def finish():
        give.wait()

        @pl.loop(1, jnp.minimum(z, most_up) + 1)
        def _(step):
            across_whole(0, step).wait()

        @pl.loop(jnp.maximum(chips - z, 1), most_down + 1)
        def _(step):
            across_whole(1, step).wait()

        spread = (
            lax.broadcasted_iota(jnp.int32, (listed_slots, wide), 1) // KB
            == lax.broadcasted_iota(jnp.int32, (listed_slots, wide), 0)
        ).astype(jnp.float32)
        ids = sel[...]
        safe = jnp.where(ids < 0, 1 << 20, ids)
        high = (safe // 64).astype(jnp.float32)
        low = lax.rem(safe, 64).astype(jnp.float32)
        found = jnp.dot(high, spread, preferred_element_type=jnp.float32) * 64.0 + jnp.dot(
            low, spread, preferred_element_type=jnp.float32
        )
        key_pos = found.astype(jnp.int32) * KB + lax.rem(
            lax.broadcasted_iota(jnp.int32, (blocks, wide), 1), KB
        )
        for b in range(PIECES):
            attend(b, key_pos)
            mix_ring.begin(b)
            if b:
                mix_ring.hand_on(b - 1)
        for b in range(PIECES):
            if b == 0:
                mix_ring.hand_on(PIECES - 1)
            mix_ring.arrived(b)
            mix(b)

    attend_at = jnp.minimum(z, most_up)

    @pl.loop(0, most_up + 1)
    def _(step):
        for piece in range(PIECES):
            @pl.when((step > 0) & comes_up(step))
            def _():
                send_up(step, piece).wait_recv()

                @pl.when(goes_up(step + 1))
                def _():
                    send_up(step + 1, piece).start()

                across(0, step, piece).start()

            @pl.when((step > 0) & comes_down(step))
            def _():
                send_down(step, piece, False, False).wait_recv()
                wrapped = z + step >= chips
                onward = step < most_down

                @pl.when(onward & wrapped)
                def _():
                    send_down(step + 1, piece, False, False).start()

                @pl.when(onward & jnp.logical_not(wrapped) & (z > 0))
                def _():
                    send_down(step + 1, piece, True, True).start()

                @pl.when(onward & (z == 0))
                def _():
                    send_down(step + 1, piece, True, False).start()

                @pl.when(wrapped)
                def _():
                    across(1, step, piece).start()

        @pl.when(step == attend_at)
        def _():
            finish()

        @pl.when((step == 0) & (z == 0))
        def _():
            pl.semaphore_wait(go, 1)
            for piece in range(PIECES):
                send_down(1, piece, False, False).start()

    for chunk in range(PIECES):
        ring.sent(chunk)
        mix_ring.sent(chunk)

    @pl.loop(1, most_up + 1)
    def _(step):
        for piece in range(PIECES):
            @pl.when(goes_up(step))
            def _():
                send_up(step, piece).wait_send()

            @pl.when(goes_down(step))
            def _():
                send_down(step, piece, False, False).wait_send()


def reach(chips):
    most_up = chips // 2 + 1
    return most_up, chips - 1 - most_up


def layer(tokens, gain, w_query, w_key, w_value, w_out, cosine, sine, select):
    rows, width = tokens.shape
    devices = lax.axis_size("kv")
    tp = lax.axis_size("tp")
    q_cols, k_cols = w_query.shape[1], w_key.shape[1]
    most_up, most_down = reach(devices // 2)
    dma = pltpu.SemaphoreType.DMA
    bf16 = jnp.bfloat16
    vmem = pl.BlockSpec(memory_space=pltpu.VMEM)
    hbm = pl.BlockSpec(memory_space=pl.ANY)
    smem = pl.BlockSpec(memory_space=pltpu.SMEM)
    return pl.pallas_call(
        layer_kernel,
        out_shape=jax.ShapeDtypeStruct((rows, w_out.shape[1]), bf16),
        in_specs=[vmem, vmem, hbm, hbm, hbm, vmem, vmem, vmem, smem, vmem],
        out_specs=vmem,
        scratch_shapes=[
            pltpu.VMEM((tp, rows, width), bf16),
            pltpu.VMEM((tp * width, q_cols + 2 * k_cols), bf16),
            pltpu.VMEM((rows, q_cols), bf16),
            pltpu.VMEM((devices * rows // KB, KB, 2 * k_cols), bf16),
            pltpu.VMEM((most_down * rows // KB, KB, 2 * k_cols), bf16),
            pltpu.VMEM((select.shape[1] * KB, 2 * k_cols), bf16),
            pltpu.VMEM((rows, q_cols), bf16),
            pltpu.VMEM((tp, rows, q_cols), bf16),
            dma((PIECES, 4)),
            dma((PIECES, 4)),
            dma((2, most_up + 1, PIECES)),
            dma((2, most_up + 1, PIECES)),
            dma((2, most_up + 1)),
            dma((2, most_up + 1)),
            dma((PIECES, 4)),
            dma((PIECES, 4)),
            dma((4,)),
            pltpu.SemaphoreType.REGULAR,
        ],
        compiler_params=pltpu.CompilerParams(collective_id=0, has_side_effects=True),
        name="layer",
    )(tokens, gain, w_query, w_key, w_value, w_out, cosine, sine, select, select)


def per_device(tokens, gain, w_query, w_key, w_value, w_out, select):
    rows = tokens.shape[0]
    positions = lax.axis_index("kv") * rows + jnp.arange(rows, dtype=jnp.int32)
    cosine, sine = rotary_tables(positions)
    return layer(
        tokens, gain.reshape(1, -1), w_query, w_key, w_value, w_out, cosine, sine, select
    )


def solution(mesh):
    placed = (
        P(("grp", "kv"), "tp"),
        P(),
        P(None, "tp"),
        P(None, "tp"),
        P(None, "tp"),
        P(None, "tp"),
        P(("grp", "kv"), None),
    )
    return jax.shard_map(
        per_device, mesh=mesh, in_specs=placed, out_specs=P(("grp", "kv"), "tp"), check_vma=False
    )
```

time: 295 us -> 167 us (0.57)
  waiting for transfers between devices: 194 us -> 0 us
  Pallas kernels: 0 us -> 162 us
  local copies, waits for them, and re-layouts: 49.4 us -> 2.47 us
  blocking collectives: 18.2 us -> 0 us
  between operations: 13.6 us -> 0.03 us
  matrix products: 7.03 us -> 0 us
  starting transfers between devices: 5.12 us -> 0 us
  other arithmetic: 6.52 us -> 2 us
    all_gather x1 -> x0, waiting for transfers between devices: 179 us -> none  [side_by_side(): lax.all_gather(both, axis, axis=dim, tiled=True)]
    pallas_call x0 -> x1, Pallas kernels: none -> 162 us  [layer(): pl.pallas_call(layer_kernel, out_shape=jax.ShapeDtypeStruct((rows, w_out....]
    split x3 -> x0, local copies, waits for them, and re-layouts: 34.6 us -> none  [side_by_side(): jnp.split(lax.all_gather(both, axis, axis=dim, tiled=True), ends, axis=al...]
    all_to_all x1 -> x0, blocking collectives: 18.2 us -> none  [sent_to_all(): return lax.all_to_all(copies, axis, split_axis=0, concat_axis=0, tiled=True)]
    all_to_all x1 -> x0, waiting for transfers between devices: 15.3 us -> none  [sent_to_all(): return lax.all_to_all(copies, axis, split_axis=0, concat_axis=0, tiled=True)]
    gather x2 -> x0, local copies, waits for them, and re-layouts: 8.27 us -> none  [the longest x1 4.14 us: per_device(): jnp.take(table_v, safe_ids, axis=0)]
    dot_general x6 -> x0, matrix products: 7.03 us -> none  [the longest x1 2.35 us: per_device(): acc_q = jnp.dot(scaled, w_query, preferred_element_type=jnp.float32)]
    all_to_all x1 -> x0, starting transfers between devices: 5.12 us -> none  [sent_to_all(): return lax.all_to_all(copies, axis, split_axis=0, concat_axis=0, tiled=True)]
  transfers between devices with their start and end apart: 2 -> 0, of which waited for: 2 -> 0; matrix products, arithmetic and copies ran while one was open for 2% -> 0% of each run, Pallas kernels for 0% -> 0%
where the time goes in v2:
time: 167 us; the launch traced here: 166 us
  Pallas kernels  162 us (97%)
  local copies, waits for them, and re-layouts  2.47 us (1%)
  other arithmetic  2 us (1%)
    pallas_call x1, Pallas kernels, layer(): pl.pallas_call(layer_kernel, out_shape=jax.ShapeDtypeStruct((rows, w_out....  162 us

profile of v2, /device:TPU:33, one launch (start us, length us, event | category | flops | bytes accessed | tf_op | source)
XLA Modules:
  0.0 166.0 jit_solution(1622595506298903184)
XLA Ops:
  0.0 1.0 fusion
  1.0 0.0 copy-start
  1.0 1.0 pad_maximum_fusion
  2.0 0.0 copy-done
  2.0 0.6 reshape.15.gain
  2.6 161.5 %layer.1 = bf16[512,512]{1,0:T(8,128)(2,1)} custom-call(bf16[512,512]{1,0:T(8,128)(2,1)} %tok.1, bf16[1,2048]{1,0:T(2,128)(2,1)} %reshape.15.gain, bf16[2048,256]{1,0:T(8,128)(2,1)} %wq.1, bf16[2048,128]{1,0:T(8,128)(2,1)} %wk.1, bf16[2048,128]{1,0:T(8,128)(2,1)} %wv.1, bf16[1024,512]{1,0:T(8,128)(2,1)} %w_out.1, f32[512,128]{1,0:T(8,128)} %get-tuple-element.8.cos, ...), custom_call_target="tpu_custom_call" | custom-call | tf_op jit(solution)/shard_map/layer/pallas_call | solution.py:376
  164.1 1.9 %copy.9 = bf16[512,512]{1,0:T(8,128)(2,1)} copy(bf16[512,512]{1,0:T(8,128)(2,1)} %layer.1) | data formatting | bytes 1048576
  (2 shorter events, 0.0 us)
Async XLA Ops:
  1.0 1.0 copy-start

commit v3 on v2

--- a/solution.py
+++ b/solution.py
@@ -11,6 +11,8 @@
 QB = 128
 KB = 32
 PIECES = 4
+IN_FLIGHT = 4
+FAR_FIRST = 6
 
 epsilon = 1e-06
 theta = 10000.0
@@ -73,7 +75,7 @@
 
 def layer_kernel(
     tok, gain, wq, wk, wv, w_out, cos, sin, listed, sel, out,
-    slots, weights, queries, need, transit, keys, attended, mixing,
+    slots, weights, queries, need, keys, attended, mixing,
     send_t, recv_t, send_z, recv_z, send_c, recv_c, send_m, recv_m, local, go,
 ):
     rows, width = tok.shape
@@ -101,30 +103,44 @@
         load.start()
 
     barrier = pltpu.get_barrier_semaphore()
+    end = chips - 1
+    last = end * 2 + core
 
     def hail(**where):
         pl.semaphore_signal(barrier, inc=1, device_id=where, device_id_type=MESH)
+
+    def let_go(chip):
+        pl.semaphore_signal(go, inc=1, device_id={"kv": chip * 2 + core}, device_id_type=MESH)
 
     hail(tp=ring.right)
     hail(tp=ring.left)
     hail(kv=partner)
-    hail(kv=down)
-
-    @pl.when(z < chips - 1)
-    def _():
-        hail(kv=up)
+
+    @pl.when(z > 0)
+    def _():
+        hail(kv=mine - 2)
+
+    @pl.when(z < end)
+    def _():
+        hail(kv=mine + 2)
+
+    @pl.when(z < most_down)
+    def _():
+        hail(kv=last)
 
     @pl.when(z == 0)
     def _():
         pl.semaphore_wait(barrier, 4)
 
-    @pl.when(z > 0)
+    @pl.when((z > 0) & (z < end))
     def _():
         pl.semaphore_wait(barrier, 5)
 
-    @pl.when(z == chips - 1)
-    def _():
-        pl.semaphore_signal(go, inc=1, device_id={"kv": up}, device_id_type=MESH)
+    @pl.when(z == end)
+    def _():
+        pl.semaphore_wait(barrier, 4 + most_down)
+        for chip in range(IN_FLIGHT):
+            let_go(chip)
 
     own_blocks = rows // KB
     chunk_blocks = chunk_rows // KB
@@ -136,29 +152,29 @@
         return pl.ds(holder * own_blocks + piece * chunk_blocks, chunk_blocks)
 
     def goes_up(step):
-        return (step <= most_up) & (z - step + 1 >= 0) & (z < chips - 1)
+        return (step <= most_up) & (z - step + 1 >= 0) & (z < end)
 
     def comes_up(step):
         return (step <= most_up) & (z - step >= 0)
 
+    def comes_down(step):
+        return (step <= most_down) & (z + step >= chips)
+
     def goes_down(step):
-        return (step <= most_down) & (lax.rem(z + step - 1, chips) < most_down)
-
-    def comes_down(step):
-        return (step <= most_down) & (lax.rem(z + step, chips) < most_down)
+        return (step <= most_down) & (z + step > chips)
 
     def send_up(step, piece):
         block = need.at[piece_blocks(lax.rem(z - step + 1 + chips, chips) * 2 + core, piece)]
         return remote(block, block, send_z.at[0, step, piece], recv_z.at[0, step, piece], kv=up)
 
-    def send_down(step, piece, from_transit, to_transit):
-        chip = lax.rem(z + step - 1, chips)
-        kept = need.at[piece_blocks(chip * 2 + core, piece)]
-        passing = transit.at[piece_blocks(lax.rem(chip, most_down), piece)]
-        return remote(
-            passing if from_transit else kept, passing if to_transit else kept,
-            send_z.at[1, step, piece], recv_z.at[1, step, piece], kv=down,
-        )
+    def send_down(step, piece):
+        block = need.at[piece_blocks(lax.rem(z + step - 1, chips) * 2 + core, piece)]
+        return remote(block, block, send_z.at[1, step, piece], recv_z.at[1, step, piece], kv=down)
+
+    def send_far(piece):
+        block = need.at[piece_blocks(mine, piece)]
+        step = jnp.minimum(z + 1, most_down)
+        return remote(block, block, send_z.at[1, step, piece], recv_z.at[1, step, piece], kv=last)
 
     def across(direction, step, piece):
         chip = lax.rem(z - step + chips, chips) if direction == 0 else lax.rem(z + step, chips)
@@ -203,9 +219,16 @@
         def _():
             send_up(1, chunk).start()
 
-        @pl.when(goes_down(1) & (z > 0))
-        def _():
-            send_down(1, chunk, False, True).start()
+    def hand_up(step, piece):
+        @pl.when(comes_up(step))
+        def _():
+            send_up(step, piece).wait_recv()
+
+            @pl.when(goes_up(step + 1))
+            def _():
+                send_up(step + 1, piece).start()
+
+            across(0, step, piece).start()
 
     ring.begin(0)
     ring.begin(1)
@@ -221,6 +244,8 @@
             ring.hand_on(chunk + 1)
         ring.arrived(chunk)
         project(chunk)
+        for step in range(1, chunk + 1):
+            hand_up(step, chunk - step)
     give = across_whole(0, 0)
     give.start()
 
@@ -296,54 +321,52 @@
 
     attend_at = jnp.minimum(z, most_up)
 
+    def go_far():
+        pl.semaphore_wait(go, 1)
+        for piece in range(PIECES):
+            send_far(piece).start()
+
     @pl.loop(0, most_up + 1)
     def _(step):
         for piece in range(PIECES):
-            @pl.when((step > 0) & comes_up(step))
+            @pl.when((step > 0) & (step + piece >= PIECES))
             def _():
-                send_up(step, piece).wait_recv()
-
-                @pl.when(goes_up(step + 1))
-                def _():
-                    send_up(step + 1, piece).start()
-
-                across(0, step, piece).start()
+                hand_up(step, piece)
 
             @pl.when((step > 0) & comes_down(step))
             def _():
-                send_down(step, piece, False, False).wait_recv()
-                wrapped = z + step >= chips
-                onward = step < most_down
-
-                @pl.when(onward & wrapped)
+                send_down(step, piece).wait_recv()
+
+                @pl.when(goes_down(step + 1))
                 def _():
-                    send_down(step + 1, piece, False, False).start()
-
-                @pl.when(onward & jnp.logical_not(wrapped) & (z > 0))
-                def _():
-                    send_down(step + 1, piece, True, True).start()
-
-                @pl.when(onward & (z == 0))
-                def _():
-                    send_down(step + 1, piece, True, False).start()
-
-                @pl.when(wrapped)
-                def _():
-                    across(1, step, piece).start()
+                    send_down(step + 1, piece).start()
+
+                across(1, step, piece).start()
+
+        @pl.when((step > 0) & (step + IN_FLIGHT <= most_down) & (z == end))
+        def _():
+            let_go(jnp.minimum(step + IN_FLIGHT - 1, most_down - 1))
+
+        @pl.when((step == attend_at) & (z >= FAR_FIRST) & (z < most_down))
+        def _():
+            go_far()
 
         @pl.when(step == attend_at)
         def _():
             finish()
 
-        @pl.when((step == 0) & (z == 0))
-        def _():
-            pl.semaphore_wait(go, 1)
-            for piece in range(PIECES):
-                send_down(1, piece, False, False).start()
+        @pl.when((step == attend_at) & (z < FAR_FIRST))
+        def _():
+            go_far()
 
     for chunk in range(PIECES):
         ring.sent(chunk)
         mix_ring.sent(chunk)
+
+    @pl.when(z < most_down)
+    def _():
+        for piece in range(PIECES):
+            send_far(piece).wait_send()
 
     @pl.loop(1, most_up + 1)
     def _(step):
@@ -352,13 +375,13 @@
             def _():
                 send_up(step, piece).wait_send()
 
-            @pl.when(goes_down(step))
+            @pl.when(goes_down(step) & (step > 1))
             def _():
-                send_down(step, piece, False, False).wait_send()
+                send_down(step, piece).wait_send()
 
 
 def reach(chips):
-    most_up = chips // 2 + 1
+    most_up = chips // 2
     return most_up, chips - 1 - most_up
 
 
@@ -383,7 +406,6 @@
             pltpu.VMEM((tp * width, q_cols + 2 * k_cols), bf16),
             pltpu.VMEM((rows, q_cols), bf16),
             pltpu.VMEM((devices * rows // KB, KB, 2 * k_cols), bf16),
-            pltpu.VMEM((most_down * rows // KB, KB, 2 * k_cols), bf16),
             pltpu.VMEM((select.shape[1] * KB, 2 * k_cols), bf16),
             pltpu.VMEM((rows, q_cols), bf16),
             pltpu.VMEM((tp, rows, q_cols), bf16),

time: 167 us -> 192 us (1.15)
  the two profiles are of different devices: /device:TPU:33 before, /device:TPU:2018 now
where the time goes in v3:
time: 192 us
  Pallas kernels  188 us (98%)
  local copies, waits for them, and re-layouts  2.47 us (1%)
  other arithmetic  2 us (1%)
    pallas_call x1, Pallas kernels, layer(): pl.pallas_call(layer_kernel, out_shape=jax.ShapeDtypeStruct((rows, w_out....  188 us

profile of v3, /device:TPU:2018, one launch (start us, length us, event | category | flops | bytes accessed | tf_op | source)
XLA Modules:
  0.0 192.0 jit_solution(2369240967691461505)
XLA Ops:
  0.0 1.0 fusion
  1.0 0.0 copy-start
  1.0 1.0 pad_maximum_fusion
  2.0 0.0 copy-done
  2.0 0.6 reshape.15.gain
  2.6 187.5 %layer.1 = bf16[512,512]{1,0:T(8,128)(2,1)} custom-call(bf16[512,512]{1,0:T(8,128)(2,1)} %tok.1, bf16[1,2048]{1,0:T(2,128)(2,1)} %reshape.15.gain, bf16[2048,256]{1,0:T(8,128)(2,1)} %wq.1, bf16[2048,128]{1,0:T(8,128)(2,1)} %wk.1, bf16[2048,128]{1,0:T(8,128)(2,1)} %wv.1, bf16[1024,512]{1,0:T(8,128)(2,1)} %w_out.1, f32[512,128]{1,0:T(8,128)} %get-tuple-element.8.cos, ...), custom_call_target="tpu_custom_call" | custom-call | tf_op jit(solution)/shard_map/layer/pallas_call | solution.py:399
  190.2 1.9 copy.9
  (2 shorter events, 0.0 us)
Async XLA Ops:
  1.0 1.0 copy-start

commit v4 on v3

--- a/solution.py
+++ b/solution.py
@@ -11,8 +11,8 @@
 QB = 128
 KB = 32
 PIECES = 4
-IN_FLIGHT = 4
-FAR_FIRST = 6
+IN_FLIGHT = 8
+DOWN_LAG = 1
 
 epsilon = 1e-06
 theta = 10000.0
@@ -333,31 +333,30 @@
             def _():
                 hand_up(step, piece)
 
-            @pl.when((step > 0) & comes_down(step))
+        down_step = step - DOWN_LAG
+
+        for piece in range(PIECES):
+            @pl.when((down_step > 0) & comes_down(down_step))
             def _():
-                send_down(step, piece).wait_recv()
-
-                @pl.when(goes_down(step + 1))
+                send_down(down_step, piece).wait_recv()
+
+                @pl.when(goes_down(down_step + 1))
                 def _():
-                    send_down(step + 1, piece).start()
-
-                across(1, step, piece).start()
-
-        @pl.when((step > 0) & (step + IN_FLIGHT <= most_down) & (z == end))
+                    send_down(down_step + 1, piece).start()
+
+                across(1, down_step, piece).start()
+
+        @pl.when((down_step > 0) & (down_step + IN_FLIGHT <= most_down) & (z == end))
         def _():
-            let_go(jnp.minimum(step + IN_FLIGHT - 1, most_down - 1))
-
-        @pl.when((step == attend_at) & (z >= FAR_FIRST) & (z < most_down))
+            let_go(jnp.minimum(down_step + IN_FLIGHT - 1, most_down - 1))
+
+        @pl.when((step == attend_at) & (z < most_down))
         def _():
             go_far()
 
         @pl.when(step == attend_at)
         def _():
             finish()
-
-        @pl.when((step == attend_at) & (z < FAR_FIRST))
-        def _():
-            go_far()
 
     for chunk in range(PIECES):
         ring.sent(chunk)

time: 192 us -> 172 us (0.90)
  the two profiles are of different devices: /device:TPU:2018 before, /device:TPU:1888 now
where the time goes in v4:
time: 172 us; the launch traced here: 171 us
  Pallas kernels  167 us (97%)
  local copies, waits for them, and re-layouts  2.47 us (1%)
  other arithmetic  2 us (1%)
    pallas_call x1, Pallas kernels, layer(): pl.pallas_call(layer_kernel, out_shape=jax.ShapeDtypeStruct((rows, w_out....  167 us

profile of v4, /device:TPU:1888, one launch (start us, length us, event | category | flops | bytes accessed | tf_op | source)
XLA Modules:
  0.0 171.5 jit_solution(2279477142866493874)
XLA Ops:
  0.0 1.0 fusion
  1.0 0.0 copy-start
  1.0 1.0 pad_maximum_fusion
  2.0 0.0 copy-done
  2.0 0.6 reshape.15.gain
  2.6 167.0 %layer.1 = bf16[512,512]{1,0:T(8,128)(2,1)} custom-call(bf16[512,512]{1,0:T(8,128)(2,1)} %tok.1, bf16[1,2048]{1,0:T(2,128)(2,1)} %reshape.15.gain, bf16[2048,256]{1,0:T(8,128)(2,1)} %wq.1, bf16[2048,128]{1,0:T(8,128)(2,1)} %wk.1, bf16[2048,128]{1,0:T(8,128)(2,1)} %wv.1, bf16[1024,512]{1,0:T(8,128)(2,1)} %w_out.1, f32[512,128]{1,0:T(8,128)} %get-tuple-element.8.cos, ...), custom_call_target="tpu_custom_call" | custom-call | tf_op jit(solution)/shard_map/layer/pallas_call | solution.py:398
  169.6 1.9 %copy.9 = bf16[512,512]{1,0:T(8,128)(2,1)} copy(bf16[512,512]{1,0:T(8,128)(2,1)} %layer.1) | data formatting | bytes 1048576
  (2 shorter events, 0.0 us)
Async XLA Ops:
  1.0 1.0 copy-start

commit v5 on v4

--- a/solution.py
+++ b/solution.py
@@ -11,7 +11,6 @@
 QB = 128
 KB = 32
 PIECES = 4
-IN_FLIGHT = 8
 DOWN_LAG = 1
 
 epsilon = 1e-06
@@ -139,8 +138,7 @@
     @pl.when(z == end)
     def _():
         pl.semaphore_wait(barrier, 4 + most_down)
-        for chip in range(IN_FLIGHT):
-            let_go(chip)
+        let_go(0)
 
     own_blocks = rows // KB
     chunk_blocks = chunk_rows // KB
@@ -325,6 +323,11 @@
         pl.semaphore_wait(go, 1)
         for piece in range(PIECES):
             send_far(piece).start()
+        send_far(0).wait_send()
+
+        @pl.when(z < most_down - 1)
+        def _():
+            let_go(z + 1)
 
     @pl.loop(0, most_up + 1)
     def _(step):
@@ -346,17 +349,17 @@
 
                 across(1, down_step, piece).start()
 
-        @pl.when((down_step > 0) & (down_step + IN_FLIGHT <= most_down) & (z == end))
-        def _():
-            let_go(jnp.minimum(down_step + IN_FLIGHT - 1, most_down - 1))
-
-        @pl.when((step == attend_at) & (z < most_down))
+        @pl.when((step == attend_at) & (z == 0))
         def _():
             go_far()
 
         @pl.when(step == attend_at)
         def _():
             finish()
+
+        @pl.when((step == attend_at) & (z > 0) & (z < most_down))
+        def _():
+            go_far()
 
     for chunk in range(PIECES):
         ring.sent(chunk)
@@ -364,7 +367,7 @@
 
     @pl.when(z < most_down)
     def _():
-        for piece in range(PIECES):
+        for piece in range(1, PIECES):
             send_far(piece).wait_send()
 
     @pl.loop(1, most_up + 1)

time: 172 us -> 219 us (1.27)
  the two profiles are of different devices: /device:TPU:1888 before, /device:TPU:1890 now
where the time goes in v5:
time: 219 us
  Pallas kernels  215 us (98%)
  local copies, waits for them, and re-layouts  2.47 us (1%)
    pallas_call x1, Pallas kernels, layer(): pl.pallas_call(layer_kernel, out_shape=jax.ShapeDtypeStruct((rows, w_out....  215 us

profile of v5, /device:TPU:1890, one launch (start us, length us, event | category | flops | bytes accessed | tf_op | source)
XLA Modules:
  0.0 219.1 jit_solution(11524568362820567683)
XLA Ops:
  0.0 1.0 fusion
  1.0 0.0 copy-start
  1.0 1.0 pad_maximum_fusion
  2.0 0.0 copy-done
  2.0 0.6 reshape.15.gain
  2.6 214.6 %layer.1 = bf16[512,512]{1,0:T(8,128)(2,1)} custom-call(bf16[512,512]{1,0:T(8,128)(2,1)} %tok.1, bf16[1,2048]{1,0:T(2,128)(2,1)} %reshape.15.gain, bf16[2048,256]{1,0:T(8,128)(2,1)} %wq.1, bf16[2048,128]{1,0:T(8,128)(2,1)} %wk.1, bf16[2048,128]{1,0:T(8,128)(2,1)} %wv.1, bf16[1024,512]{1,0:T(8,128)(2,1)} %w_out.1, f32[512,128]{1,0:T(8,128)} %get-tuple-element.8.cos, ...), custom_call_target="tpu_custom_call" | custom-call | tf_op jit(solution)/shard_map/layer/pallas_call | solution.py:401
  217.3 1.9 copy.9
  (2 shorter events, 0.0 us)
Async XLA Ops:
  1.0 1.0 copy-start

commit v6 on v4

--- a/solution.py
+++ b/solution.py
@@ -11,8 +11,7 @@
 QB = 128
 KB = 32
 PIECES = 4
-IN_FLIGHT = 8
-DOWN_LAG = 1
+MOST_LAG = 4
 
 epsilon = 1e-06
 theta = 10000.0
@@ -139,7 +138,7 @@
     @pl.when(z == end)
     def _():
         pl.semaphore_wait(barrier, 4 + most_down)
-        for chip in range(IN_FLIGHT):
+        for chip in range(most_down):
             let_go(chip)
 
     own_blocks = rows // KB
@@ -319,21 +318,23 @@
             mix_ring.arrived(b)
             mix(b)
 
-    attend_at = jnp.minimum(z, most_up)
+    first = most_up + 1
+    lag = (jnp.maximum(z - first, 0) * MOST_LAG) // (end - first)
+    attend_at = jnp.where(z < first, z, jnp.maximum(most_up, most_down + lag))
 
     def go_far():
         pl.semaphore_wait(go, 1)
         for piece in range(PIECES):
             send_far(piece).start()
 
-    @pl.loop(0, most_up + 1)
+    @pl.loop(0, most_down + MOST_LAG + 1)
     def _(step):
         for piece in range(PIECES):
             @pl.when((step > 0) & (step + piece >= PIECES))
             def _():
                 hand_up(step, piece)
 
-        down_step = step - DOWN_LAG
+        down_step = step - lag
 
         for piece in range(PIECES):
             @pl.when((down_step > 0) & comes_down(down_step))
@@ -345,10 +346,6 @@
                     send_down(down_step + 1, piece).start()
 
                 across(1, down_step, piece).start()
-
-        @pl.when((down_step > 0) & (down_step + IN_FLIGHT <= most_down) & (z == end))
-        def _():
-            let_go(jnp.minimum(down_step + IN_FLIGHT - 1, most_down - 1))
 
         @pl.when((step == attend_at) & (z < most_down))
         def _():

time: 172 us -> 224 us (1.30)
  the two profiles are of different devices: /device:TPU:1888 before, /device:TPU:1824 now
where the time goes in v6:
time: 224 us
  Pallas kernels  220 us (98%)
  local copies, waits for them, and re-layouts  2.47 us (1%)
    pallas_call x1, Pallas kernels, layer(): pl.pallas_call(layer_kernel, out_shape=jax.ShapeDtypeStruct((rows, w_out....  220 us

profile of v6, /device:TPU:1824, one launch (start us, length us, event | category | flops | bytes accessed | tf_op | source)
XLA Modules:
  0.0 224.1 jit_solution(12975858008898764552)
XLA Ops:
  0.0 1.0 fusion
  1.0 0.0 copy-start
  1.0 1.0 pad_maximum_fusion
  2.0 0.0 copy-done
  2.0 0.6 reshape.15.gain
  2.6 219.6 %layer.1 = bf16[512,512]{1,0:T(8,128)(2,1)} custom-call(bf16[512,512]{1,0:T(8,128)(2,1)} %tok.1, bf16[1,2048]{1,0:T(2,128)(2,1)} %reshape.15.gain, bf16[2048,256]{1,0:T(8,128)(2,1)} %wq.1, bf16[2048,128]{1,0:T(8,128)(2,1)} %wk.1, bf16[2048,128]{1,0:T(8,128)(2,1)} %wv.1, bf16[1024,512]{1,0:T(8,128)(2,1)} %w_out.1, f32[512,128]{1,0:T(8,128)} %get-tuple-element.8.cos, ...), custom_call_target="tpu_custom_call" | custom-call | tf_op jit(solution)/shard_map/layer/pallas_call | solution.py:395
  222.2 1.9 copy.9
  (2 shorter events, 0.0 us)
Async XLA Ops:
  1.0 1.0 copy-start

commit v7 on v5

--- a/solution.py
+++ b/solution.py
@@ -11,7 +11,7 @@
 QB = 128
 KB = 32
 PIECES = 4
-DOWN_LAG = 1
+FAR_FIRST = 9
 
 epsilon = 1e-06
 theta = 10000.0
@@ -317,7 +317,9 @@
             mix_ring.arrived(b)
             mix(b)
 
-    attend_at = jnp.minimum(z, most_up)
+    first = most_up + 1
+    lag = 1 + (jnp.maximum(z - first, 0) * 2) // (end - first)
+    attend_at = jnp.where(z < first, z, jnp.maximum(most_up, most_down + lag))
 
     def go_far():
         pl.semaphore_wait(go, 1)
@@ -329,14 +331,14 @@
         def _():
             let_go(z + 1)
 
-    @pl.loop(0, most_up + 1)
+    @pl.loop(0, most_down + 4)
     def _(step):
         for piece in range(PIECES):
             @pl.when((step > 0) & (step + piece >= PIECES))
             def _():
                 hand_up(step, piece)
 
-        down_step = step - DOWN_LAG
+        down_step = step - lag
 
         for piece in range(PIECES):
             @pl.when((down_step > 0) & comes_down(down_step))
@@ -349,7 +351,7 @@
 
                 across(1, down_step, piece).start()
 
-        @pl.when((step == attend_at) & (z == 0))
+        @pl.when((step == attend_at) & (z < FAR_FIRST))
         def _():
             go_far()
 
@@ -357,7 +359,7 @@
         def _():
             finish()
 
-        @pl.when((step == attend_at) & (z > 0) & (z < most_down))
+        @pl.when((step == attend_at) & (z >= FAR_FIRST) & (z < most_down))
         def _():
             go_far()
 

time: 219 us -> 192 us (0.88)
  the two profiles are of different devices: /device:TPU:1890 before, /device:TPU:1888 now
where the time goes in v7:
time: 192 us
  Pallas kernels  187 us (97%)
  local copies, waits for them, and re-layouts  2.47 us (1%)
  other arithmetic  2 us (1%)
    pallas_call x1, Pallas kernels, layer(): pl.pallas_call(layer_kernel, out_shape=jax.ShapeDtypeStruct((rows, w_out....  187 us

profile of v7, /device:TPU:1888, one launch (start us, length us, event | category | flops | bytes accessed | tf_op | source)
XLA Modules:
  0.0 192.0 jit_solution(12191106220111068775)
XLA Ops:
  0.0 1.0 fusion
  1.0 0.0 copy-start
  1.0 1.0 pad_maximum_fusion
  2.0 0.0 copy-done
  2.0 0.6 reshape.15.gain
  2.6 187.5 %layer.1 = bf16[512,512]{1,0:T(8,128)(2,1)} custom-call(bf16[512,512]{1,0:T(8,128)(2,1)} %tok.1, bf16[1,2048]{1,0:T(2,128)(2,1)} %reshape.15.gain, bf16[2048,256]{1,0:T(8,128)(2,1)} %wq.1, bf16[2048,128]{1,0:T(8,128)(2,1)} %wk.1, bf16[2048,128]{1,0:T(8,128)(2,1)} %wv.1, bf16[1024,512]{1,0:T(8,128)(2,1)} %w_out.1, f32[512,128]{1,0:T(8,128)} %get-tuple-element.8.cos, ...), custom_call_target="tpu_custom_call" | custom-call | tf_op jit(solution)/shard_map/layer/pallas_call | solution.py:403
  190.1 1.9 copy.9
  (2 shorter events, 0.0 us)
Async XLA Ops:
  1.0 1.0 copy-start

commit v8 on v2

--- a/solution.py
+++ b/solution.py
@@ -207,6 +207,17 @@
         def _():
             send_down(1, chunk, False, True).start()
 
+    def hand_up(step, piece):
+        @pl.when(comes_up(step))
+        def _():
+            send_up(step, piece).wait_recv()
+
+            @pl.when(goes_up(step + 1))
+            def _():
+                send_up(step + 1, piece).start()
+
+            across(0, step, piece).start()
+
     ring.begin(0)
     ring.begin(1)
     for load in loads:
@@ -221,6 +232,8 @@
             ring.hand_on(chunk + 1)
         ring.arrived(chunk)
         project(chunk)
+        for step in range(1, chunk + 1):
+            hand_up(step, chunk - step)
     give = across_whole(0, 0)
     give.start()
 
@@ -258,7 +271,7 @@
             )
         out[at, :] = total.astype(jnp.bfloat16)
 
-    def finish():
+    def all_here():
         give.wait()
 
         @pl.loop(1, jnp.minimum(z, most_up) + 1)
@@ -269,6 +282,7 @@
         def _(step):
             across_whole(1, step).wait()
 
+    def key_positions():
         spread = (
             lax.broadcasted_iota(jnp.int32, (listed_slots, wide), 1) // KB
             == lax.broadcasted_iota(jnp.int32, (listed_slots, wide), 0)
@@ -283,31 +297,30 @@
         key_pos = found.astype(jnp.int32) * KB + lax.rem(
             lax.broadcasted_iota(jnp.int32, (blocks, wide), 1), KB
         )
-        for b in range(PIECES):
-            attend(b, key_pos)
-            mix_ring.begin(b)
-            if b:
-                mix_ring.hand_on(b - 1)
-        for b in range(PIECES):
-            if b == 0:
+        return key_pos
+
+    def stage(which):
+        if which == 0:
+            all_here()
+        if which < PIECES:
+            attend(which, key_positions())
+            mix_ring.begin(which)
+            if which:
+                mix_ring.hand_on(which - 1)
+        else:
+            if which == PIECES:
                 mix_ring.hand_on(PIECES - 1)
-            mix_ring.arrived(b)
-            mix(b)
+            mix_ring.arrived(which - PIECES)
+            mix(which - PIECES)
 
     attend_at = jnp.minimum(z, most_up)
 
-    @pl.loop(0, most_up + 1)
+    @pl.loop(0, most_up + 2 * PIECES)
     def _(step):
         for piece in range(PIECES):
-            @pl.when((step > 0) & comes_up(step))
-            def _():
-                send_up(step, piece).wait_recv()
-
-                @pl.when(goes_up(step + 1))
-                def _():
-                    send_up(step + 1, piece).start()
-
-                across(0, step, piece).start()
+            @pl.when((step > 0) & (step + piece >= PIECES))
+            def _():
+                hand_up(step, piece)
 
             @pl.when((step > 0) & comes_down(step))
             def _():
@@ -330,16 +343,17 @@
                 @pl.when(wrapped)
                 def _():
                     across(1, step, piece).start()
-
-        @pl.when(step == attend_at)
-        def _():
-            finish()
 
         @pl.when((step == 0) & (z == 0))
         def _():
             pl.semaphore_wait(go, 1)
             for piece in range(PIECES):
                 send_down(1, piece, False, False).start()
+
+        for which in range(2 * PIECES):
+            @pl.when(step == attend_at + which)
+            def _():
+                stage(which)
 
     for chunk in range(PIECES):
         ring.sent(chunk)

time: 167 us -> 150 us (0.90)
  Pallas kernels: 162 us -> 145 us
    pallas_call x1, Pallas kernels: 162 us -> 145 us  [layer(): pl.pallas_call(layer_kernel, out_shape=jax.ShapeDtypeStruct((rows, w_out....]
where the time goes in v8:
time: 150 us
  Pallas kernels  145 us (97%)
  local copies, waits for them, and re-layouts  2.47 us (2%)
  other arithmetic  2 us (1%)
    pallas_call x1, Pallas kernels, layer(): pl.pallas_call(layer_kernel, out_shape=jax.ShapeDtypeStruct((rows, w_out....  145 us

profile of v8, /device:TPU:33, one launch (start us, length us, event | category | flops | bytes accessed | tf_op | source)
XLA Modules:
  0.0 149.9 jit_solution(6950631277501382656)
XLA Ops:
  0.0 1.0 fusion
  1.0 0.0 copy-start
  1.0 1.0 pad_maximum_fusion
  2.0 0.0 copy-done
  2.0 0.6 reshape.15.gain
  2.6 145.4 %layer.1 = bf16[512,512]{1,0:T(8,128)(2,1)} custom-call(bf16[512,512]{1,0:T(8,128)(2,1)} %tok.1, bf16[1,2048]{1,0:T(2,128)(2,1)} %reshape.15.gain, bf16[2048,256]{1,0:T(8,128)(2,1)} %wq.1, bf16[2048,128]{1,0:T(8,128)(2,1)} %wk.1, bf16[2048,128]{1,0:T(8,128)(2,1)} %wv.1, bf16[1024,512]{1,0:T(8,128)(2,1)} %w_out.1, f32[512,128]{1,0:T(8,128)} %get-tuple-element.8.cos, ...), custom_call_target="tpu_custom_call" | custom-call | tf_op jit(solution)/shard_map/layer/pallas_call | solution.py:390
  148.0 1.9 %copy.9 = bf16[512,512]{1,0:T(8,128)(2,1)} copy(bf16[512,512]{1,0:T(8,128)(2,1)} %layer.1) | data formatting | bytes 1048576
  (2 shorter events, 0.0 us)
Async XLA Ops:
  1.0 1.0 copy-start

commit v9 on v8

--- a/solution.py
+++ b/solution.py
@@ -17,11 +17,12 @@
 MESH = pl.DeviceIdType.MESH
 
 
-def rotary_tables(positions):
-    frequency = theta ** (-jnp.arange(0, HD, 2, dtype=jnp.float32) / HD)
+def rotary_table(positions):
+    half = HD // 2
+    column = jnp.arange(HD, dtype=jnp.int32)
+    frequency = theta ** (-(2 * (column % half)).astype(jnp.float32) / HD)
     angles = positions.astype(jnp.float32)[:, None] * frequency[None, :]
-    cosine, sine = jnp.cos(angles), jnp.sin(angles)
-    return jnp.concatenate([cosine, cosine], 1), jnp.concatenate([-sine, sine], 1)
+    return jnp.where((column < half)[None, :], jnp.cos(angles), jnp.sin(angles))
 
 
 def remote(src, dst, send, recv, **where):
@@ -72,7 +73,7 @@
 
 
 def layer_kernel(
-    tok, gain, wq, wk, wv, w_out, cos, sin, listed, sel, out,
+    tok, gain, wq, wk, wv, w_out, table, listed, sel, out,
     slots, weights, queries, need, transit, keys, attended, mixing,
     send_t, recv_t, send_z, recv_z, send_c, recv_c, send_m, recv_m, local, go,
 ):
@@ -81,7 +82,7 @@
     chunk_rows = rows // PIECES
     devices = lax.axis_size("kv")
     chips = devices // 2
-    most_up, most_down = reach(chips)
+    most_up, most_down = reach(chips, 0)[0], reach(chips, PIECES - 1)[1]
     mine = lax.axis_index("kv")
     z, core = mine // 2, lax.rem(mine, 2)
     partner = mine + 1 - 2 * core
@@ -135,17 +136,19 @@
     def piece_blocks(holder, piece):
         return pl.ds(holder * own_blocks + piece * chunk_blocks, chunk_blocks)
 
-    def goes_up(step):
-        return (step <= most_up) & (z - step + 1 >= 0) & (z < chips - 1)
-
-    def comes_up(step):
-        return (step <= most_up) & (z - step >= 0)
-
-    def goes_down(step):
-        return (step <= most_down) & (lax.rem(z + step - 1, chips) < most_down)
-
-    def comes_down(step):
-        return (step <= most_down) & (lax.rem(z + step, chips) < most_down)
+    def goes_up(step, piece):
+        return (step <= reach(chips, piece)[0]) & (z - step + 1 >= 0) & (z < chips - 1)
+
+    def comes_up(step, piece):
+        return (step <= reach(chips, piece)[0]) & (z - step >= 0)
+
+    def goes_down(step, piece):
+        far = reach(chips, piece)[1]
+        return (step <= far) & (lax.rem(z + step - 1, chips) < far)
+
+    def comes_down(step, piece):
+        far = reach(chips, piece)[1]
+        return (step <= far) & (lax.rem(z + step, chips) < far)
 
     def send_up(step, piece):
         block = need.at[piece_blocks(lax.rem(z - step + 1 + chips, chips) * 2 + core, piece)]
@@ -167,11 +170,13 @@
             block, block, send_c.at[direction, step], recv_c.at[direction, step], kv=partner
         )
 
-    def across_whole(direction, step):
-        block = need.at[pl.ds(mine * own_blocks, own_blocks)]
+    def across_whole(direction, step, share=1):
+        block = need.at[pl.ds(mine * own_blocks, own_blocks // share)]
         return remote(
             block, block, send_c.at[direction, step], recv_c.at[direction, step], kv=partner
         )
+
+    gain_row = gain[...].astype(jnp.float32).reshape(1, -1)
 
     def project(chunk):
         at = piece_rows(chunk)
@@ -180,14 +185,17 @@
         for t in range(tp):
             block = slots[t, at, :].astype(jnp.float32)
             squares += jnp.sum(block * block, axis=1, keepdims=True)
-            scaled = (block * gain[:, t * width:(t + 1) * width].astype(jnp.float32)).astype(
+            scaled = (block * gain_row[:, t * width:(t + 1) * width]).astype(
                 jnp.bfloat16
             )
             total += jnp.dot(
                 scaled, weights[t * width:(t + 1) * width, :], preferred_element_type=jnp.float32
             )
         total *= lax.rsqrt(squares / (tp * width) + epsilon)
-        cosine, sine = cos[at, :], sin[at, :]
+        turns = table[at, :]
+        swapped = pltpu.roll(turns, HD // 2, 1)
+        front = lax.broadcasted_iota(jnp.int32, turns.shape, 1) < HD // 2
+        cosine, sine = jnp.where(front, turns, swapped), jnp.where(front, -swapped, turns)
         heads = []
         for h in range((q_cols + k_cols) // HD):
             head = total[:, h * HD:(h + 1) * HD]
@@ -199,20 +207,20 @@
         need[kept, :, 0:k_cols] = heads[-1].reshape(chunk_blocks, KB, k_cols)
         need[kept, :, k_cols:2 * k_cols] = values.reshape(chunk_blocks, KB, k_cols)
 
-        @pl.when(goes_up(1))
+        @pl.when(goes_up(1, chunk))
         def _():
             send_up(1, chunk).start()
 
-        @pl.when(goes_down(1) & (z > 0))
+        @pl.when(goes_down(1, chunk) & (z > 0))
         def _():
             send_down(1, chunk, False, True).start()
 
     def hand_up(step, piece):
-        @pl.when(comes_up(step))
+        @pl.when(comes_up(step, piece))
         def _():
             send_up(step, piece).wait_recv()
 
-            @pl.when(goes_up(step + 1))
+            @pl.when(goes_up(step + 1, piece))
             def _():
                 send_up(step + 1, piece).start()
 
@@ -274,13 +282,18 @@
     def all_here():
         give.wait()
 
-        @pl.loop(1, jnp.minimum(z, most_up) + 1)
+        @pl.loop(1, jnp.minimum(z, most_up - 1) + 1)
         def _(step):
             across_whole(0, step).wait()
 
-        @pl.loop(jnp.maximum(chips - z, 1), most_down + 1)
+        @pl.loop(jnp.maximum(chips - z, 1), most_down)
         def _(step):
             across_whole(1, step).wait()
+
+        @pl.when(z >= most_up)
+        def _():
+            across_whole(0, most_up, 2).wait()
+            across_whole(1, most_down, 2).wait()
 
     def key_positions():
         spread = (
@@ -322,11 +335,11 @@
             def _():
                 hand_up(step, piece)
 
-            @pl.when((step > 0) & comes_down(step))
+            @pl.when((step > 0) & comes_down(step, piece))
             def _():
                 send_down(step, piece, False, False).wait_recv()
                 wrapped = z + step >= chips
-                onward = step < most_down
+                onward = step < reach(chips, piece)[1]
 
                 @pl.when(onward & wrapped)
                 def _():
@@ -362,26 +375,27 @@
     @pl.loop(1, most_up + 1)
     def _(step):
         for piece in range(PIECES):
-            @pl.when(goes_up(step))
+            @pl.when(goes_up(step, piece))
             def _():
                 send_up(step, piece).wait_send()
 
-            @pl.when(goes_down(step))
+            @pl.when(goes_down(step, piece))
             def _():
                 send_down(step, piece, False, False).wait_send()
 
 
-def reach(chips):
-    most_up = chips // 2 + 1
+def reach(chips, piece):
+    most_up = chips // 2 + 1 + (piece < PIECES // 2)
     return most_up, chips - 1 - most_up
 
 
-def layer(tokens, gain, w_query, w_key, w_value, w_out, cosine, sine, select):
+def layer(tokens, gain, w_query, w_key, w_value, w_out, table, select):
     rows, width = tokens.shape
     devices = lax.axis_size("kv")
     tp = lax.axis_size("tp")
     q_cols, k_cols = w_query.shape[1], w_key.shape[1]
-    most_up, most_down = reach(devices // 2)
+    chips = devices // 2
+    most_up, most_down = reach(chips, 0)[0], reach(chips, PIECES - 1)[1]
     dma = pltpu.SemaphoreType.DMA
     bf16 = jnp.bfloat16
     vmem = pl.BlockSpec(memory_space=pltpu.VMEM)
@@ -390,7 +404,7 @@
     return pl.pallas_call(
         layer_kernel,
         out_shape=jax.ShapeDtypeStruct((rows, w_out.shape[1]), bf16),
-        in_specs=[vmem, vmem, hbm, hbm, hbm, vmem, vmem, vmem, smem, vmem],
+        in_specs=[vmem, vmem, hbm, hbm, hbm, vmem, vmem, smem, vmem],
         out_specs=vmem,
         scratch_shapes=[
             pltpu.VMEM((tp, rows, width), bf16),
@@ -414,15 +428,15 @@
         ],
         compiler_params=pltpu.CompilerParams(collective_id=0, has_side_effects=True),
         name="layer",
-    )(tokens, gain, w_query, w_key, w_value, w_out, cosine, sine, select, select)
+    )(tokens, gain, w_query, w_key, w_value, w_out, table, select, select)
 
 
 def per_device(tokens, gain, w_query, w_key, w_value, w_out, select):
     rows = tokens.shape[0]
     positions = lax.axis_index("kv") * rows + jnp.arange(rows, dtype=jnp.int32)
-    cosine, sine = rotary_tables(positions)
+    table = rotary_table(positions)
     return layer(
-        tokens, gain.reshape(1, -1), w_query, w_key, w_value, w_out, cosine, sine, select
+        tokens, gain, w_query, w_key, w_value, w_out, table, select
     )
 
 

time: 150 us -> 147 us (0.980)
  Pallas kernels: 145 us -> 143 us
    pallas_call x1, Pallas kernels: 145 us -> 143 us  [layer(): pl.pallas_call(layer_kernel, out_shape=jax.ShapeDtypeStruct((rows, w_out....]
    select_n x0 -> x1, other arithmetic: none -> 1.78 us  [rotary_table(): return jnp.where((column < half)[None, :], jnp.cos(angles), jnp.sin(angles))]
where the time goes in v9:
time: 147 us; the launch traced here: 146 us
  Pallas kernels  143 us (97%)
  local copies, waits for them, and re-layouts  1.87 us (1%)
  other arithmetic  1.8 us (1%)
    pallas_call x1, Pallas kernels, layer(): pl.pallas_call(layer_kernel, out_shape=jax.ShapeDtypeStruct((rows, w_out....  143 us

profile of v9, /device:TPU:33, one launch (start us, length us, event | category | flops | bytes accessed | tf_op | source)
XLA Modules:
  0.0 146.4 jit_solution(7805567220553155533)
XLA Ops:
  0.0 1.8 %fusion.table = f32[512,128]{1,0:T(8,128)} fusion(f32[128]{0:T(128)S(1)} %fusion.5, f32[512]{0:T(512)S(1)} %add_convert_fusion, pred[128]{0:T(512)(128)(4,1)S(1)} %iota_compare_fusion), kind=kLoop, calls=%fused_computation.2 | loop fusion | flops 131072 | bytes 264832 | tf_op jit(solution)/shard_map/jit(_where)/select_n | solution.py:25
  1.8 142.7 %layer.1 = bf16[512,512]{1,0:T(8,128)(2,1)} custom-call(bf16[512,512]{1,0:T(8,128)(2,1)} %tok.1, bf16[2048]{0:T(1024)(128)(2,1)} %gain.1, bf16[2048,256]{1,0:T(8,128)(2,1)} %wq.1, bf16[2048,128]{1,0:T(8,128)(2,1)} %wk.1, bf16[2048,128]{1,0:T(8,128)(2,1)} %wv.1, bf16[1024,512]{1,0:T(8,128)(2,1)} %w_out.1, f32[512,128]{1,0:T(8,128)} %fusion.table, ...), custom_call_target="tpu_custom_call" | custom-call | tf_op jit(solution)/shard_map/layer/pallas_call | solution.py:404
  144.6 1.9 %copy.9 = bf16[512,512]{1,0:T(8,128)(2,1)} copy(bf16[512,512]{1,0:T(8,128)(2,1)} %layer.1) | data formatting | bytes 1048576
  (3 shorter events, 0.0 us)

commit v10 on v8

--- a/solution.py
+++ b/solution.py
@@ -11,6 +11,7 @@
 QB = 128
 KB = 32
 PIECES = 4
+DIRECT = 2
 
 epsilon = 1e-06
 theta = 10000.0
@@ -20,8 +21,7 @@
 def rotary_tables(positions):
     frequency = theta ** (-jnp.arange(0, HD, 2, dtype=jnp.float32) / HD)
     angles = positions.astype(jnp.float32)[:, None] * frequency[None, :]
-    cosine, sine = jnp.cos(angles), jnp.sin(angles)
-    return jnp.concatenate([cosine, cosine], 1), jnp.concatenate([-sine, sine], 1)
+    return jnp.cos(angles), jnp.sin(angles)
 
 
 def remote(src, dst, send, recv, **where):
@@ -74,7 +74,7 @@
 def layer_kernel(
     tok, gain, wq, wk, wv, w_out, cos, sin, listed, sel, out,
     slots, weights, queries, need, transit, keys, attended, mixing,
-    send_t, recv_t, send_z, recv_z, send_c, recv_c, send_m, recv_m, local, go,
+    send_t, recv_t, send_z, recv_z, send_c, recv_c, send_m, recv_m, send_d, local, go,
 ):
     rows, width = tok.shape
     tp = lax.axis_size("tp")
@@ -114,17 +114,27 @@
     def _():
         hail(kv=up)
 
+    last = (chips - 1) * 2 + core
+
+    @pl.when((z > 0) & (z <= DIRECT))
+    def _():
+        hail(kv=last)
+
     @pl.when(z == 0)
     def _():
         pl.semaphore_wait(barrier, 4)
 
-    @pl.when(z > 0)
+    @pl.when((z > 0) & (z < chips - 1))
     def _():
         pl.semaphore_wait(barrier, 5)
 
     @pl.when(z == chips - 1)
     def _():
-        pl.semaphore_signal(go, inc=1, device_id={"kv": up}, device_id_type=MESH)
+        pl.semaphore_wait(barrier, 5 + DIRECT)
+        for chip in range(DIRECT + 1):
+            pl.semaphore_signal(
+                go, inc=1, device_id={"kv": chip * 2 + core}, device_id_type=MESH
+            )
 
     own_blocks = rows // KB
     chunk_blocks = chunk_rows // KB
@@ -135,17 +145,22 @@
     def piece_blocks(holder, piece):
         return pl.ds(holder * own_blocks + piece * chunk_blocks, chunk_blocks)
 
+    def by_relay(at):
+        return (at == 0) | (at > DIRECT)
+
     def goes_up(step):
-        return (step <= most_up) & (z - step + 1 >= 0) & (z < chips - 1)
+        return (step <= reach(chips)[0]) & (z - step + 1 >= 0) & (z < chips - 1)
 
     def comes_up(step):
-        return (step <= most_up) & (z - step >= 0)
+        return (step <= reach(chips)[0]) & (z - step >= 0)
 
     def goes_down(step):
-        return (step <= most_down) & (lax.rem(z + step - 1, chips) < most_down)
+        far = reach(chips)[1]
+        return (step <= far) & (lax.rem(z + step - 1, chips) < far) & by_relay(z + step - 1)
 
     def comes_down(step):
-        return (step <= most_down) & (lax.rem(z + step, chips) < most_down)
+        far = reach(chips)[1]
+        return (step <= far) & (lax.rem(z + step, chips) < far) & by_relay(z + step)
 
     def send_up(step, piece):
         block = need.at[piece_blocks(lax.rem(z - step + 1 + chips, chips) * 2 + core, piece)]
@@ -160,6 +175,11 @@
             send_z.at[1, step, piece], recv_z.at[1, step, piece], kv=down,
         )
 
+    def send_direct(piece):
+        block = need.at[piece_blocks(mine, piece)]
+        step = lax.rem(z, DIRECT + 1) + 1
+        return remote(block, block, send_d.at[piece], recv_z.at[1, step, piece], kv=last)
+
     def across(direction, step, piece):
         chip = lax.rem(z - step + chips, chips) if direction == 0 else lax.rem(z + step, chips)
         block = need.at[piece_blocks(chip * 2 + core, piece)]
@@ -172,6 +192,8 @@
         return remote(
             block, block, send_c.at[direction, step], recv_c.at[direction, step], kv=partner
         )
+
+    gain_row = gain[...].astype(jnp.float32).reshape(1, -1)
 
     def project(chunk):
         at = piece_rows(chunk)
@@ -180,14 +202,15 @@
         for t in range(tp):
             block = slots[t, at, :].astype(jnp.float32)
             squares += jnp.sum(block * block, axis=1, keepdims=True)
-            scaled = (block * gain[:, t * width:(t + 1) * width].astype(jnp.float32)).astype(
+            scaled = (block * gain_row[:, t * width:(t + 1) * width]).astype(
                 jnp.bfloat16
             )
             total += jnp.dot(
                 scaled, weights[t * width:(t + 1) * width, :], preferred_element_type=jnp.float32
             )
         total *= lax.rsqrt(squares / (tp * width) + epsilon)
-        cosine, sine = cos[at, :], sin[at, :]
+        c, n = cos[at, :], sin[at, :]
+        cosine, sine = jnp.concatenate([c, c], 1), jnp.concatenate([-n, n], 1)
         heads = []
         for h in range((q_cols + k_cols) // HD):
             head = total[:, h * HD:(h + 1) * HD]
@@ -232,8 +255,12 @@
             ring.hand_on(chunk + 1)
         ring.arrived(chunk)
         project(chunk)
-        for step in range(1, chunk + 1):
-            hand_up(step, chunk - step)
+
+        @pl.when(z >= PIECES)
+        def _():
+            for step in range(1, chunk + 1):
+                hand_up(step, chunk - step)
+
     give = across_whole(0, 0)
     give.start()
 
@@ -318,7 +345,7 @@
     @pl.loop(0, most_up + 2 * PIECES)
     def _(step):
         for piece in range(PIECES):
-            @pl.when((step > 0) & (step + piece >= PIECES))
+            @pl.when((step > 0) & ((step + piece >= PIECES) | (z < PIECES)))
             def _():
                 hand_up(step, piece)
 
@@ -326,7 +353,7 @@
             def _():
                 send_down(step, piece, False, False).wait_recv()
                 wrapped = z + step >= chips
-                onward = step < most_down
+                onward = step < reach(chips)[1]
 
                 @pl.when(onward & wrapped)
                 def _():
@@ -350,6 +377,12 @@
             for piece in range(PIECES):
                 send_down(1, piece, False, False).start()
 
+        @pl.when((step == 0) & (z > 0) & (z <= DIRECT))
+        def _():
+            pl.semaphore_wait(go, 1)
+            for piece in range(PIECES):
+                send_direct(piece).start()
+
         for which in range(2 * PIECES):
             @pl.when(step == attend_at + which)
             def _():
@@ -358,6 +391,11 @@
     for chunk in range(PIECES):
         ring.sent(chunk)
         mix_ring.sent(chunk)
+
+    @pl.when((z > 0) & (z <= DIRECT))
+    def _():
+        for piece in range(PIECES):
+            send_direct(piece).wait_send()
 
     @pl.loop(1, most_up + 1)
     def _(step):
@@ -376,12 +414,13 @@
     return most_up, chips - 1 - most_up
 
 
-def layer(tokens, gain, w_query, w_key, w_value, w_out, cosine, sine, select):
+def layer(tokens, gain, w_query, w_key, w_value, w_out, tables, select):
     rows, width = tokens.shape
     devices = lax.axis_size("kv")
     tp = lax.axis_size("tp")
     q_cols, k_cols = w_query.shape[1], w_key.shape[1]
-    most_up, most_down = reach(devices // 2)
+    chips = devices // 2
+    most_up, most_down = reach(chips)
     dma = pltpu.SemaphoreType.DMA
     bf16 = jnp.bfloat16
     vmem = pl.BlockSpec(memory_space=pltpu.VMEM)
@@ -409,20 +448,21 @@
             dma((2, most_up + 1)),
             dma((PIECES, 4)),
             dma((PIECES, 4)),
+            dma((PIECES,)),
             dma((4,)),
             pltpu.SemaphoreType.REGULAR,
         ],
         compiler_params=pltpu.CompilerParams(collective_id=0, has_side_effects=True),
         name="layer",
-    )(tokens, gain, w_query, w_key, w_value, w_out, cosine, sine, select, select)
+    )(tokens, gain, w_query, w_key, w_value, w_out, *tables, select, select)
 
 
 def per_device(tokens, gain, w_query, w_key, w_value, w_out, select):
     rows = tokens.shape[0]
     positions = lax.axis_index("kv") * rows + jnp.arange(rows, dtype=jnp.int32)
-    cosine, sine = rotary_tables(positions)
+    tables = rotary_tables(positions)
     return layer(
-        tokens, gain.reshape(1, -1), w_query, w_key, w_value, w_out, cosine, sine, select
+        tokens, gain, w_query, w_key, w_value, w_out, tables, select
     )
 
 

time: 150 us -> 144 us (0.960)
  Pallas kernels: 145 us -> 140 us
    pallas_call x1, Pallas kernels: 145 us -> 140 us  [layer(): pl.pallas_call(layer_kernel, out_shape=jax.ShapeDtypeStruct((rows, w_out....]
    sin x0 -> x1, other arithmetic: none -> 1.81 us  [rotary_tables(): return (jnp.cos(angles), jnp.sin(angles))]
where the time goes in v10:
time: 144 us
  Pallas kernels  140 us (97%)
  local copies, waits for them, and re-layouts  1.87 us (1%)
  other arithmetic  1.83 us (1%)
    pallas_call x1, Pallas kernels, layer(): pl.pallas_call(layer_kernel, out_shape=jax.ShapeDtypeStruct((rows, w_out....  140 us

profile of v10, /device:TPU:33, one launch (start us, length us, event | category | flops | bytes accessed | tf_op | source)
XLA Modules:
  0.0 143.9 jit_solution(616545966277218409)
XLA Ops:
  0.0 1.8 %multiply_sine_fusion = (f32[512,64]{1,0:T(8,128)}, f32[512,64]{1,0:T(8,128)}) fusion(f32[64]{0:T(128)S(1)} %multiply_power_fusion, f32[512]{0:T(512)S(1)} %add_convert_fusion), kind=kLoop, calls=%fused_computation | loop fusion | flops 32768 | bytes 264448 | tf_op jit(solution)/shard_map/sin | solution.py:24
  1.8 140.2 %layer.1 = bf16[512,512]{1,0:T(8,128)(2,1)} custom-call(bf16[512,512]{1,0:T(8,128)(2,1)} %tok.1, bf16[2048]{0:T(1024)(128)(2,1)} %gain.1, bf16[2048,256]{1,0:T(8,128)(2,1)} %wq.1, bf16[2048,128]{1,0:T(8,128)(2,1)} %wk.1, bf16[2048,128]{1,0:T(8,128)(2,1)} %wv.1, bf16[1024,512]{1,0:T(8,128)(2,1)} %w_out.1, f32[512,64]{1,0:T(8,128)} %get-tuple-element.6.cos, ...), custom_call_target="tpu_custom_call" | custom-call | tf_op jit(solution)/shard_map/layer/pallas_call | solution.py:429
  142.0 1.9 %copy.9 = bf16[512,512]{1,0:T(8,128)(2,1)} copy(bf16[512,512]{1,0:T(8,128)(2,1)} %layer.1) | data formatting | bytes 1048576
  (2 shorter events, 0.0 us)

commit v11 on v10

--- a/solution.py
+++ b/solution.py
@@ -11,7 +11,7 @@
 QB = 128
 KB = 32
 PIECES = 4
-DIRECT = 2
+DIRECT = 3
 
 epsilon = 1e-06
 theta = 10000.0
@@ -349,27 +349,30 @@
             def _():
                 hand_up(step, piece)
 
-            @pl.when((step > 0) & comes_down(step))
-            def _():
-                send_down(step, piece, False, False).wait_recv()
-                wrapped = z + step >= chips
-                onward = step < reach(chips)[1]
+        down_step = step - jnp.where(z > most_up, 1, 0)
+
+        for piece in range(PIECES):
+            @pl.when((down_step > 0) & comes_down(down_step))
+            def _():
+                send_down(down_step, piece, False, False).wait_recv()
+                wrapped = z + down_step >= chips
+                onward = down_step < reach(chips)[1]
 
                 @pl.when(onward & wrapped)
                 def _():
-                    send_down(step + 1, piece, False, False).start()
+                    send_down(down_step + 1, piece, False, False).start()
 
                 @pl.when(onward & jnp.logical_not(wrapped) & (z > 0))
                 def _():
-                    send_down(step + 1, piece, True, True).start()
+                    send_down(down_step + 1, piece, True, True).start()
 
                 @pl.when(onward & (z == 0))
                 def _():
-                    send_down(step + 1, piece, True, False).start()
+                    send_down(down_step + 1, piece, True, False).start()
 
                 @pl.when(wrapped)
                 def _():
-                    across(1, step, piece).start()
+                    across(1, down_step, piece).start()
 
         @pl.when((step == 0) & (z == 0))
         def _():

time: 144 us -> 143 us (level)
  the two profiles are of different devices: /device:TPU:33 before, /device:TPU:2016 now
where the time goes in v11:
time: 143 us
  Pallas kernels  139 us (97%)
  local copies, waits for them, and re-layouts  1.87 us (1%)
  other arithmetic  1.83 us (1%)
    pallas_call x1, Pallas kernels, layer(): pl.pallas_call(layer_kernel, out_shape=jax.ShapeDtypeStruct((rows, w_out....  139 us

profile of v11, /device:TPU:2016, one launch (start us, length us, event | category | flops | bytes accessed | tf_op | source)
XLA Modules:
  0.0 142.6 jit_solution(3574818365450945079)
XLA Ops:
  0.0 1.8 %multiply_sine_fusion = (f32[512,64]{1,0:T(8,128)}, f32[512,64]{1,0:T(8,128)}) fusion(f32[64]{0:T(128)S(1)} %multiply_power_fusion, f32[512]{0:T(512)S(1)} %add_convert_fusion), kind=kLoop, calls=%fused_computation | loop fusion | flops 32768 | bytes 264448 | tf_op jit(solution)/shard_map/sin | solution.py:24
  1.8 138.9 %layer.1 = bf16[512,512]{1,0:T(8,128)(2,1)} custom-call(bf16[512,512]{1,0:T(8,128)(2,1)} %tok.1, bf16[2048]{0:T(1024)(128)(2,1)} %gain.1, bf16[2048,256]{1,0:T(8,128)(2,1)} %wq.1, bf16[2048,128]{1,0:T(8,128)(2,1)} %wk.1, bf16[2048,128]{1,0:T(8,128)(2,1)} %wv.1, bf16[1024,512]{1,0:T(8,128)(2,1)} %w_out.1, f32[512,64]{1,0:T(8,128)} %get-tuple-element.6.cos, ...), custom_call_target="tpu_custom_call" | custom-call | tf_op jit(solution)/shard_map/layer/pallas_call | solution.py:432
  140.7 1.9 %copy.9 = bf16[512,512]{1,0:T(8,128)(2,1)} copy(bf16[512,512]{1,0:T(8,128)(2,1)} %layer.1) | data formatting | bytes 1048576
  (2 shorter events, 0.0 us)

commit v12 on v11

--- a/solution.py
+++ b/solution.py
@@ -73,7 +73,7 @@
 
 def layer_kernel(
     tok, gain, wq, wk, wv, w_out, cos, sin, listed, sel, out,
-    slots, weights, queries, need, transit, keys, attended, mixing,
+    slots, weights, queries, need, transit, keys, places, attended, mixing,
     send_t, recv_t, send_z, recv_z, send_c, recv_c, send_m, recv_m, send_d, local, go,
 ):
     rows, width = tok.shape
@@ -241,73 +241,9 @@
 
             across(0, step, piece).start()
 
-    ring.begin(0)
-    ring.begin(1)
-    for load in loads:
-        load.wait()
-    for chunk in range(PIECES):
-        if chunk == 0:
-            ring.hand_on(0)
-            ring.begin(2)
-            ring.hand_on(1)
-            ring.begin(3)
-        elif chunk + 1 < PIECES:
-            ring.hand_on(chunk + 1)
-        ring.arrived(chunk)
-        project(chunk)
-
-        @pl.when(z >= PIECES)
-        def _():
-            for step in range(1, chunk + 1):
-                hand_up(step, chunk - step)
-
-    give = across_whole(0, 0)
-    give.start()
-
     blocks, listed_slots = sel.shape
     wide = listed_slots * KB
     heads_here = q_cols // HD
-
-    def attend(b, key_pos):
-        @pl.loop(0, listed_slots, unroll=4)
-        def _(s):
-            keys[pl.ds(pl.multiple_of(s * KB, KB), KB), :] = need[jnp.maximum(listed[b, s], 0)]
-
-        q_pos = mine * rows + b * QB + lax.broadcasted_iota(jnp.int32, (QB, wide), 0)
-        allowed = jnp.broadcast_to(key_pos[b:b + 1, :], (QB, wide)) <= q_pos
-        for h in range(heads_here):
-            score = lax.dot_general(
-                queries[b * QB:(b + 1) * QB, h * HD:(h + 1) * HD], keys[:, 0:HD],
-                (((1,), (1,)), ((), ())), preferred_element_type=jnp.float32,
-            ) * HD ** (-0.5)
-            score = jnp.where(allowed, score, -jnp.inf)
-            raised = jnp.exp(score - jnp.max(score, axis=1, keepdims=True))
-            parts = (raised / jnp.sum(raised, axis=1, keepdims=True)).astype(jnp.bfloat16)
-            attended[b * QB:(b + 1) * QB, h * HD:(h + 1) * HD] = jnp.dot(
-                parts, keys[:, HD:2 * HD], preferred_element_type=jnp.float32
-            ).astype(jnp.bfloat16)
-        mixing[mix_ring.me, b * QB:(b + 1) * QB, :] = attended[b * QB:(b + 1) * QB, :]
-
-    def mix(chunk):
-        at = piece_rows(chunk)
-        total = jnp.zeros((chunk_rows, out.shape[1]), jnp.float32)
-        for t in range(tp):
-            total += jnp.dot(
-                mixing[t, at, :], w_out[t * q_cols:(t + 1) * q_cols, :],
-                preferred_element_type=jnp.float32,
-            )
-        out[at, :] = total.astype(jnp.bfloat16)
-
-    def all_here():
-        give.wait()
-
-        @pl.loop(1, jnp.minimum(z, most_up) + 1)
-        def _(step):
-            across_whole(0, step).wait()
-
-        @pl.loop(jnp.maximum(chips - z, 1), most_down + 1)
-        def _(step):
-            across_whole(1, step).wait()
 
     def key_positions():
         spread = (
@@ -326,11 +262,77 @@
         )
         return key_pos
 
+    ring.begin(0)
+    ring.begin(1)
+    places[...] = key_positions()
+    for load in loads:
+        load.wait()
+    for chunk in range(PIECES):
+        if chunk == 0:
+            ring.hand_on(0)
+            ring.begin(2)
+            ring.hand_on(1)
+            ring.begin(3)
+        elif chunk + 1 < PIECES:
+            ring.hand_on(chunk + 1)
+        ring.arrived(chunk)
+        project(chunk)
+
+        @pl.when(z >= PIECES)
+        def _():
+            for step in range(1, chunk + 1):
+                hand_up(step, chunk - step)
+
+    give = across_whole(0, 0)
+    give.start()
+
+
+    def attend(b, key_pos):
+        @pl.loop(0, listed_slots, unroll=4)
+        def _(s):
+            keys[pl.ds(pl.multiple_of(s * KB, KB), KB), :] = need[jnp.maximum(listed[b, s], 0)]
+
+        q_pos = mine * rows + b * QB + lax.broadcasted_iota(jnp.int32, (QB, wide), 0)
+        allowed = jnp.broadcast_to(key_pos[b:b + 1, :], (QB, wide)) <= q_pos
+        for h in range(heads_here):
+            score = lax.dot_general(
+                queries[b * QB:(b + 1) * QB, h * HD:(h + 1) * HD], keys[:, 0:HD],
+                (((1,), (1,)), ((), ())), preferred_element_type=jnp.float32,
+            ) * HD ** (-0.5)
+            score = jnp.where(allowed, score, -jnp.inf)
+            raised = jnp.exp(score - jnp.max(score, axis=1, keepdims=True))
+            parts = (raised * (1.0 / jnp.sum(raised, axis=1, keepdims=True))).astype(jnp.bfloat16)
+            attended[b * QB:(b + 1) * QB, h * HD:(h + 1) * HD] = jnp.dot(
+                parts, keys[:, HD:2 * HD], preferred_element_type=jnp.float32
+            ).astype(jnp.bfloat16)
+        mixing[mix_ring.me, b * QB:(b + 1) * QB, :] = attended[b * QB:(b + 1) * QB, :]
+
+    def mix(chunk):
+        at = piece_rows(chunk)
+        total = jnp.zeros((chunk_rows, out.shape[1]), jnp.float32)
+        for t in range(tp):
+            total += jnp.dot(
+                mixing[t, at, :], w_out[t * q_cols:(t + 1) * q_cols, :],
+                preferred_element_type=jnp.float32,
+            )
+        out[at, :] = total.astype(jnp.bfloat16)
+
+    def all_here():
+        give.wait()
+
+        @pl.loop(1, jnp.minimum(z, most_up) + 1)
+        def _(step):
+            across_whole(0, step).wait()
+
+        @pl.loop(jnp.maximum(chips - z, 1), most_down + 1)
+        def _(step):
+            across_whole(1, step).wait()
+
     def stage(which):
         if which == 0:
             all_here()
         if which < PIECES:
-            attend(which, key_positions())
+            attend(which, places[...])
             mix_ring.begin(which)
             if which:
                 mix_ring.hand_on(which - 1)
@@ -441,6 +443,7 @@
             pltpu.VMEM((devices * rows // KB, KB, 2 * k_cols), bf16),
             pltpu.VMEM((most_down * rows // KB, KB, 2 * k_cols), bf16),
             pltpu.VMEM((select.shape[1] * KB, 2 * k_cols), bf16),
+            pltpu.VMEM((select.shape[0], select.shape[1] * KB), jnp.int32),
             pltpu.VMEM((rows, q_cols), bf16),
             pltpu.VMEM((tp, rows, q_cols), bf16),
             dma((PIECES, 4)),

time: 143 us -> 142 us (level)
  no operation moved by 1% of the time
where the time goes in v12:
time: 142 us
  Pallas kernels  138 us (97%)
  local copies, waits for them, and re-layouts  1.87 us (1%)
  other arithmetic  1.83 us (1%)
    pallas_call x1, Pallas kernels, layer(): pl.pallas_call(layer_kernel, out_shape=jax.ShapeDtypeStruct((rows, w_out....  138 us

profile of v12, /device:TPU:2016, one launch (start us, length us, event | category | flops | bytes accessed | tf_op | source)
XLA Modules:
  0.0 142.2 jit_solution(4649677042156073289)
XLA Ops:
  0.0 1.8 %multiply_sine_fusion = (f32[512,64]{1,0:T(8,128)}, f32[512,64]{1,0:T(8,128)}) fusion(f32[64]{0:T(128)S(1)} %multiply_power_fusion, f32[512]{0:T(512)S(1)} %add_convert_fusion), kind=kLoop, calls=%fused_computation | loop fusion | flops 32768 | bytes 264448 | tf_op jit(solution)/shard_map/sin | solution.py:24
  1.8 138.5 %layer.1 = bf16[512,512]{1,0:T(8,128)(2,1)} custom-call(bf16[512,512]{1,0:T(8,128)(2,1)} %tok.1, bf16[2048]{0:T(1024)(128)(2,1)} %gain.1, bf16[2048,256]{1,0:T(8,128)(2,1)} %wq.1, bf16[2048,128]{1,0:T(8,128)(2,1)} %wk.1, bf16[2048,128]{1,0:T(8,128)(2,1)} %wv.1, bf16[1024,512]{1,0:T(8,128)(2,1)} %w_out.1, f32[512,64]{1,0:T(8,128)} %get-tuple-element.6.cos, ...), custom_call_target="tpu_custom_call" | custom-call | tf_op jit(solution)/shard_map/layer/pallas_call | solution.py:434
  140.3 1.9 %copy.9 = bf16[512,512]{1,0:T(8,128)(2,1)} copy(bf16[512,512]{1,0:T(8,128)(2,1)} %layer.1) | data formatting | bytes 1048576
  (2 shorter events, 0.0 us)

commit v13 on v12

--- a/solution.py
+++ b/solution.py
@@ -334,10 +334,12 @@
         if which < PIECES:
             attend(which, places[...])
             mix_ring.begin(which)
-            if which:
-                mix_ring.hand_on(which - 1)
+            if which > 1:
+                mix_ring.hand_on(which - 2)
         else:
             if which == PIECES:
+                mix_ring.hand_on(PIECES - 2)
+            if which == PIECES + 1:
                 mix_ring.hand_on(PIECES - 1)
             mix_ring.arrived(which - PIECES)
             mix(which - PIECES)

time: 142 us -> 140 us (0.986)
  the two profiles are of different devices: /device:TPU:2016 before, /device:TPU:33 now
where the time goes in v13:
time: 140 us; the launch traced here: 139 us
  Pallas kernels  136 us (97%)
  local copies, waits for them, and re-layouts  1.87 us (1%)
  other arithmetic  1.83 us (1%)
    pallas_call x1, Pallas kernels, layer(): pl.pallas_call(layer_kernel, out_shape=jax.ShapeDtypeStruct((rows, w_out....  136 us

profile of v13, /device:TPU:33, one launch (start us, length us, event | category | flops | bytes accessed | tf_op | source)
XLA Modules:
  0.0 139.3 jit_solution(17527402416855746048)
XLA Ops:
  0.0 1.8 %multiply_sine_fusion = (f32[512,64]{1,0:T(8,128)}, f32[512,64]{1,0:T(8,128)}) fusion(f32[64]{0:T(128)S(1)} %multiply_power_fusion, f32[512]{0:T(512)S(1)} %add_convert_fusion), kind=kLoop, calls=%fused_computation | loop fusion | flops 32768 | bytes 264448 | tf_op jit(solution)/shard_map/sin | solution.py:24
  1.8 135.5 %layer.1 = bf16[512,512]{1,0:T(8,128)(2,1)} custom-call(bf16[512,512]{1,0:T(8,128)(2,1)} %tok.1, bf16[2048]{0:T(1024)(128)(2,1)} %gain.1, bf16[2048,256]{1,0:T(8,128)(2,1)} %wq.1, bf16[2048,128]{1,0:T(8,128)(2,1)} %wk.1, bf16[2048,128]{1,0:T(8,128)(2,1)} %wv.1, bf16[1024,512]{1,0:T(8,128)(2,1)} %w_out.1, f32[512,64]{1,0:T(8,128)} %get-tuple-element.6.cos, ...), custom_call_target="tpu_custom_call" | custom-call | tf_op jit(solution)/shard_map/layer/pallas_call | solution.py:436
  137.4 1.9 %copy.9 = bf16[512,512]{1,0:T(8,128)(2,1)} copy(bf16[512,512]{1,0:T(8,128)(2,1)} %layer.1) | data formatting | bytes 1048576
  (2 shorter events, 0.0 us)
